TPU v7x, 32 devices: a whole 2x2x4 slice. The times are simulated.
32 devices in a mesh: ep: 8 (over z, x), tp: 4 (over y, core).
Axes of the slice: x: 2, y: 2, z: 4, core: 2. Of those that a mesh axis runs over, the one named last changes fastest.
Arguments:
- mixer_query: bfloat16 [2048, 2048], P('ep', 'tp'), may hold values from -6 to 6
- mixer_forget: bfloat16 [2048, 2048], P('ep', 'tp'), may hold values from -5.5 to 5.5
- mixer_value: bfloat16 [2048, 2048], P('ep', 'tp'), may hold values from -6 to 6
- mixer_gate: bfloat16 [2048, 2048], P('ep', 'tp'), may hold values from -6 to 6
- forget_floor: float32 [2048], P('tp'), may hold values from 0.88 to 1
- head_gain: float32 [128], replicated, may hold values from 0.1 to 1.9
- mixer_proj: bfloat16 [2048, 2048], P(None, 'tp'), may hold values from -0.125 to 0.125
- expert_tokens: bfloat16 [1024, 2048], P('ep'), may hold values from -6 to 6
- expert_gain: float32 [2048], replicated, may hold values from 0.1 to 1.9
- routes: int32 [1024, 2], P('ep'), may hold values from 0 to 7, as said below
- group_logits: float32 [1024, 4], P('ep'), may hold values from -6 to 6
- choice_logits: float32 [1024, 2], P('ep'), may hold values from -6 to 6
- w_gate: bfloat16 [8, 2048, 2048], P('ep', None, 'tp'), may hold values from -0.125 to 0.125
- w_up: bfloat16 [8, 2048, 2048], P('ep', None, 'tp'), may hold values from -0.125 to 0.125
- w_down: bfloat16 [8, 2048, 2048], P('ep', None, 'tp'), may hold values from -0.125 to 0.125
Outputs:
- mixer_out: bfloat16 [2048, 2048], P('ep', 'tp')
- expert_out: bfloat16 [1024, 2048], P('ep', 'tp')
Inputs may be any that keep to these rules, and one draw needn't show every extreme that they name: `routes`: in each aligned block of 128 rows (the rows of one index of ep) no expert is named by more than 64 rows, and some expert reaches that bound in every block; the 2 experts of a row differ and lie in the same group.
All inputs are finite; a program needn't handle non-finite values.
Results may differ from a plain program's by a relative error of at most 0.01.
Values may be sent and summed in bfloat16 or wider, within the bound.
A program may use at most 64 MiB of HBM per device.

v0:
```python
import jax
import jax.numpy as jnp
from jax import lax
from jax.sharding import PartitionSpec as P

KEYDIM = 128
VDIM = 128
GROUPS = 4
TOPK = 2
BLOCK = 64


norm_eps = 1e-06
highest_precision = lax.Precision.HIGHEST


def entering(shard, axis, join, neutral):
    place = lax.axis_index(axis)
    gathered = jax.tree.map(
        lambda a, kind: lax.all_gather(a.astype(kind), axis), shard, (jnp.bfloat16, jnp.bfloat16)
    )
    state = jax.tree.map(lambda a, e: jnp.zeros_like(a) + jnp.asarray(e, a.dtype), shard, neutral)

    def one(lap, state):
        return join(
            state,
            jax.tree.map(
                lambda a, own: lax.dynamic_index_in_dim(a, lap, 0, False).astype(own.dtype),
                gathered,
                shard,
            ),
        )

    return lax.fori_loop(0, place, one, state)


def rms_scale(features, gain_vec):
    return (
        features
        * lax.rsqrt(jnp.mean(features * features, axis=-1, keepdims=True) + norm_eps)
        * gain_vec
    )


def block_terms(query_block, input_block, log_blk, value_block, carried_state):
    cumulative_log = jnp.cumsum(log_blk, axis=0)
    between_block_term = jnp.einsum(
        "zug,ugr->zur",
        query_block * jnp.exp(cumulative_log),
        carried_state,
        precision=highest_precision,
    )
    causal = jnp.tril(jnp.ones((query_block.shape[0], query_block.shape[0]), dtype=bool))[
        :, :, None, None
    ]
    differ = cumulative_log[:, None] - cumulative_log[None, :]
    decays = jnp.exp(jnp.where(causal, differ, -jnp.inf))
    scores = jnp.sum(query_block[:, None] * input_block[None, :] * decays, axis=-1)
    result = between_block_term + jnp.einsum(
        "tsh,shv->thv", scores, value_block, precision=highest_precision
    )
    ending_log_decay = cumulative_log[-1]
    updated_state = jnp.exp(ending_log_decay)[..., None] * carried_state + jnp.einsum(
        "twa,twr->war",
        input_block * jnp.exp(ending_log_decay[None] - cumulative_log),
        value_block,
        precision=highest_precision,
    )
    return (updated_state, result, cumulative_log)


def mixer_local(
    mixer_query, mixer_forget, mixer_value, mixer_gate, forget_floor, head_gain, mixer_proj
):
    length = mixer_query.shape[0]
    heads_local = mixer_query.shape[1] // KEYDIM
    blocks = length // BLOCK

    def split_blocks(source_array, last_width):
        return source_array.reshape(blocks, BLOCK, heads_local, last_width)

    queries = jax.nn.silu(mixer_query.astype(jnp.float32))
    input_rates = (1.0 - forget_floor) * jax.nn.sigmoid(-mixer_forget.astype(jnp.float32))
    log_forget = jnp.log1p(-input_rates)
    value_rows = mixer_value.astype(jnp.float32)

    def advance(carry_pair, block_inputs):
        carried_state, offset_log = carry_pair
        query_block, input_block, value_block, log_blk = block_inputs
        updated_state, result, cumulative_log = block_terms(
            query_block, input_block, log_blk, value_block, carried_state
        )
        scaled_values = query_block * jnp.exp(cumulative_log + offset_log[None])
        return ((updated_state, offset_log + cumulative_log[-1]), (result, scaled_values))

    initial = (
        jnp.zeros((heads_local, KEYDIM, VDIM), jnp.float32),
        jnp.zeros((heads_local, KEYDIM), jnp.float32),
    )
    (local_state, total_log), (output_rows, scaled_values) = lax.scan(
        advance,
        initial,
        (
            split_blocks(queries, KEYDIM),
            split_blocks(input_rates, KEYDIM),
            split_blocks(value_rows, VDIM),
            split_blocks(log_forget, KEYDIM),
        ),
    )

    def combine(earlier, later):
        return (earlier[0] * later[0], later[0][..., None] * earlier[1] + later[1])

    identity = (jnp.ones_like(total_log), jnp.zeros_like(local_state))
    incoming_state = entering((jnp.exp(total_log), local_state), "ep", combine, identity)
    output_rows = output_rows + jnp.einsum(
        "qsfa,fap->qsfp", scaled_values, incoming_state[1], precision=highest_precision
    )
    output_rows = output_rows.reshape(length, heads_local, VDIM)
    gate_act = jax.nn.silu(mixer_gate.astype(jnp.float32)).reshape(length, heads_local, VDIM)
    gated_out = rms_scale(output_rows, head_gain) * gate_act
    mixed_heads = gated_out.reshape(length, heads_local * VDIM).astype(jnp.bfloat16)
    summed = jnp.dot(
        lax.all_gather(mixed_heads, "tp", axis=1, tiled=True),
        mixer_proj,
        preferred_element_type=jnp.float32,
    )
    return summed.astype(jnp.bfloat16)


def gate_weights(routes, group_logits, choice_logits, group_size):
    group_exp = jnp.exp(group_logits)
    group_prob = group_exp / jnp.sum(group_exp, axis=-1, keepdims=True)
    groups_of = routes // group_size
    member = (groups_of[..., None] == jnp.arange(GROUPS, dtype=jnp.int32)).astype(jnp.float32)
    picked_prob = jnp.sum(member * group_prob[:, None, :], axis=-1)
    choice_exp = jnp.exp(choice_logits)
    together = (groups_of[:, :, None] == groups_of[:, None, :]).astype(jnp.float32)
    within = jnp.sum(together * choice_exp[:, None, :], axis=-1)
    return picked_prob * choice_exp / within


def finish(gate_pre, up_pre, down_local, sources, slot_count):
    hidden = (jax.nn.silu(gate_pre) * up_pre).astype(jnp.bfloat16)
    summed = jnp.dot(
        lax.all_gather(hidden, "tp", axis=1, tiled=True),
        down_local,
        preferred_element_type=jnp.float32,
    )
    shaped = summed.astype(jnp.bfloat16).reshape(sources, slot_count, down_local.shape[1])
    return lax.all_to_all(shaped, "ep", split_axis=0, concat_axis=0, tiled=True)


def expert_local(
    expert_tokens, expert_gain, routes, group_logits, choice_logits, w_gate, w_up, w_down
):
    count_rows, model_width = expert_tokens.shape
    experts_all = lax.axis_size("ep")
    capacity = 2 * TOPK * count_rows // experts_all
    normed = rms_scale(expert_tokens.astype(jnp.float32), expert_gain).astype(jnp.bfloat16)
    weights = gate_weights(routes, group_logits, choice_logits, experts_all // GROUPS)
    flat_routes = routes.reshape(-1)
    onehot = (flat_routes[:, None] == jnp.arange(experts_all, dtype=jnp.int32)).astype(jnp.int32)
    earlier = jnp.cumsum(onehot, axis=0) - onehot
    ranks = jnp.sum(earlier * onehot, axis=-1)
    slot_of = flat_routes * capacity + ranks
    token_ids = jnp.arange(flat_routes.shape[0], dtype=jnp.int32) // TOPK
    token_of = jnp.full((experts_all * capacity,), count_rows, jnp.int32).at[slot_of].set(token_ids)
    padded = jnp.concatenate([normed, jnp.zeros((1, model_width), jnp.bfloat16)], axis=0)
    outgoing = padded[token_of].reshape(experts_all, capacity, model_width)
    gate_local = w_gate[0]
    up_local = w_up[0]
    down_local = w_down[0]
    arrived = lax.all_to_all(outgoing, "ep", split_axis=0, concat_axis=0, tiled=True)
    sources, slot_count, _ = arrived.shape
    flat_in = arrived.reshape(sources * slot_count, model_width)
    gate_pre = jnp.dot(flat_in, gate_local, preferred_element_type=jnp.float32)
    up_pre = jnp.dot(flat_in, up_local, preferred_element_type=jnp.float32)
    came_back = finish(gate_pre, up_pre, down_local, sources, slot_count)
    picked = (
        came_back.reshape(-1, came_back.shape[-1])[slot_of].astype(jnp.float32)
        * weights.reshape(-1)[:, None]
    )
    return jnp.sum(picked.reshape(count_rows, TOPK, -1), axis=1).astype(jnp.bfloat16)


def per_device(
    mixer_query,
    mixer_forget,
    mixer_value,
    mixer_gate,
    forget_floor,
    head_gain,
    mixer_proj,
    expert_tokens,
    expert_gain,
    routes,
    group_logits,
    choice_logits,
    w_gate,
    w_up,
    w_down,
):
    mixer_out = mixer_local(
        mixer_query, mixer_forget, mixer_value, mixer_gate, forget_floor, head_gain, mixer_proj
    )
    expert_out = expert_local(
        expert_tokens, expert_gain, routes, group_logits, choice_logits, w_gate, w_up, w_down
    )
    return (mixer_out, expert_out)


def solution(mesh):
    return jax.shard_map(
        per_device,
        mesh=mesh,
        in_specs=(
            P("ep", "tp"),
            P("ep", "tp"),
            P("ep", "tp"),
            P("ep", "tp"),
            P("tp"),
            P(),
            P(None, "tp"),
            P("ep", None),
            P(),
            P("ep", None),
            P("ep", None),
            P("ep", None),
            P("ep", None, "tp"),
            P("ep", None, "tp"),
            P("ep", None, "tp"),
        ),
        out_specs=(P("ep", "tp"), P("ep", "tp")),
        check_vma=False,
    )
```

profile of v0, /device:TPU:0, one launch (start us, length us, event | category | flops | bytes accessed | tf_op | source)
XLA Modules:
  0.0 168.5 jit_solution(13482604115918556136)
XLA Ops:
  10.3 1.4 scatter_custom_fusion
  13.0 1.2 fusion.35
  14.3 3.3 %gather_fusion = bf16[512,2048]{1,0:T(8,128)(2,1)} fusion(bf16[129,2048]{1,0:T(8,128)(2,1)S(1)} %concatenate.3, s32[1024]{0:T(1024)S(1)} %pad_clamp_fusion.1), kind=kCustom, calls=%fused_computation | custom fusion | bytes 4196352 | tf_op jit(solution)/shard_map/gather | solution.py:170
  17.6 7.4 %all-to-all-start = ((bf16[8,64,2048]{2,1,0:T(8,128)(2,1)}), bf16[8,64,2048]{2,1,0:T(8,128)(2,1)}, u32[]{:S(2)}, u32[]{:S(2)}) async-start(bf16[8,64,2048]{2,1,0:T(8,128)(2,1)} %bitcast.133), calls=%async_computation | async-start | bytes 4194304 | tf_op jit(solution)/shard_map/all_to_all | solution.py:174
  25.1 1.2 divide_multiply_fusion
  29.6 1.9 %reshape.178 = f32[4,64,4,128]{3,2,1,0:T(4,128)} reshape(bf16[256,512]{1,0:T(8,128)(2,1)} %param.21) | data formatting | bytes 786432 | tf_op jit(solution)/shard_map/reshape | solution.py:80
  31.5 37.6 %while.30 = (s32[]{:T(128)}, f32[4,128,128]{2,1,0:T(8,128)S(1)}, f32[4,128]{1,0:T(4,128)S(1)}, f32[4,64,4,128]{3,1,0,2:T(8,128)}, f32[4,64,4,128]{3,1,0,2:T(8,12...) while((s32[]{:T(128)}, f32[4,128,128]{2,1,0:T(8,128)S(1)}, ...), condition=%wide.region_3.4_spmd.clone, body=%wide.region_0.3_spmd.clone.sunk | while | flops 138826752 | bytes 5011073 | solution.py:100
  33.5 3.7 %multiply_reduce_fusion.4 = f32[64,64,4]{1,2,0:T(4,128)S(1)} fusion(f32[64,4,128]{2,0,1:T(8,128)S(1)} %copy.120, f32[64,4,128]{2,1,0:T(4,128)S(1)} %fusion.74, f32[64,4,128]{2,0,1:T(8,128)S(1)} %copy.121, f32[64,4,128]{2,1,0:T(4,128)S(1)} %get-tuple-element.314, pred[64,64]{1,0:T(8,128)(4,1)S(1)} %iota_compare_fusion.5), kind=kLoop, calls=%fused_computation.5.clone.1 | loop fusion | flops 10469376 | bytes 593920 | tf_op jit(solution)/shard_map/while/body/eval_jaxpr/reduce_sum | solution.py:58
  42.9 3.7 %multiply_reduce_fusion.4 = f32[64,64,4]{1,2,0:T(4,128)S(1)} fusion(f32[64,4,128]{2,0,1:T(8,128)S(1)} %copy.120, f32[64,4,128]{2,1,0:T(4,128)S(1)} %fusion.74, f32[64,4,128]{2,0,1:T(8,128)S(1)} %copy.121, f32[64,4,128]{2,1,0:T(4,128)S(1)} %get-tuple-element.314, pred[64,64]{1,0:T(8,128)(4,1)S(1)} %iota_compare_fusion.5), kind=kLoop, calls=%fused_computation.5.clone.1 | loop fusion | flops 10469376 | bytes 593920 | tf_op jit(solution)/shard_map/while/body/eval_jaxpr/reduce_sum | solution.py:58
  52.3 3.7 %multiply_reduce_fusion.4 = f32[64,64,4]{1,2,0:T(4,128)S(1)} fusion(f32[64,4,128]{2,0,1:T(8,128)S(1)} %copy.120, f32[64,4,128]{2,1,0:T(4,128)S(1)} %fusion.74, f32[64,4,128]{2,0,1:T(8,128)S(1)} %copy.121, f32[64,4,128]{2,1,0:T(4,128)S(1)} %get-tuple-element.314, pred[64,64]{1,0:T(8,128)(4,1)S(1)} %iota_compare_fusion.5), kind=kLoop, calls=%fused_computation.5.clone.1 | loop fusion | flops 10469376 | bytes 593920 | tf_op jit(solution)/shard_map/while/body/eval_jaxpr/reduce_sum | solution.py:58
  61.7 3.7 %multiply_reduce_fusion.4 = f32[64,64,4]{1,2,0:T(4,128)S(1)} fusion(f32[64,4,128]{2,0,1:T(8,128)S(1)} %copy.120, f32[64,4,128]{2,1,0:T(4,128)S(1)} %fusion.74, f32[64,4,128]{2,0,1:T(8,128)S(1)} %copy.121, f32[64,4,128]{2,1,0:T(4,128)S(1)} %get-tuple-element.314, pred[64,64]{1,0:T(8,128)(4,1)S(1)} %iota_compare_fusion.5), kind=kLoop, calls=%fused_computation.5.clone.1 | loop fusion | flops 10469376 | bytes 593920 | tf_op jit(solution)/shard_map/while/body/eval_jaxpr/reduce_sum | solution.py:58
  69.8 3.5 %all-to-all-done = bf16[8,64,2048]{2,1,0:T(8,128)(2,1)} async-done(((bf16[8,64,2048]{2,1,0:T(8,128)(2,1)}), bf16[8,64,2048]{2,1,0:T(8,128)(2,1)}, u32[]{:S(2)}, u32[]{:S(2)}) %all-to-all-start) | async-done | bytes 2097184 | tf_op jit(solution)/shard_map/all_to_all | solution.py:174
  73.3 3.0 %fusion.22 = f32[512,512]{1,0:T(8,128)S(1)} fusion(bf16[512,2048]{1,0:T(8,128)(2,1)} %bitcast.15, bf16[1,2048,512]{2,1,0:T(8,128)(2,1)S(1)} %copy-done), kind=kOutput, calls=%fused_computation.42 | convolution fusion | flops 1073741824 | bytes 5242880 | tf_op jit(solution)/shard_map/dot_general | solution.py:177
  76.3 3.7 %fusion.30 = bf16[512,512]{1,0:T(8,128)(2,1)} fusion(bf16[512,2048]{1,0:T(8,128)(2,1)} %bitcast.15, bf16[1,2048,512]{2,1,0:T(8,128)(2,1)S(1)} %copy-done.7, f32[512,512]{1,0:T(8,128)S(1)} %fusion.22), kind=kOutput, calls=%fused_computation.48 | convolution fusion | flops 1075314688 | bytes 5767168 | tf_op jit(solution)/shard_map/dot_general | solution.py:178
  80.2 18.7 %all-gather.2 = bf16[8,4,128]{2,1,0:T(4,128)(2,1)S(1)} all-gather(bf16[1,4,128]{2,1,0:T(4,128)(2,1)S(1)} %fusion.49), channel_id=2, replica_groups=mesh['ep'=8,'tp'=4] {'ep'}, dimensions={0}, use_global_device_ids=true | all-gather | bytes 9216 | tf_op jit(solution)/shard_map/all_gather | solution.py:20
  98.8 12.7 %all-gather.11.cloned.1.call-done = bf16[32,128,128]{2,1,0:T(8,128)(2,1)} async-done(((bf16[4,128,128]{2,1,0:T(8,128)(2,1)}), bf16[32,128,128]{2,1,0:T(8,128)(2,1)}) %all-gather.11.cloned.1.call-update) | async-done | bytes 1048592 | tf_op jit(solution)/shard_map/all_gather | solution.py:20
  111.6 1.7 %fusion.52 = f32[4,128,256]{1,2,0:S(1)} fusion(f32[4,128,128]{2,1,0:T(8,128)S(1)} %get-tuple-element.99, f32[4,128,256]{1,2,0:T(8,128)} %bitcast.138), kind=kOutput, calls=%fused_computation.106 | convolution fusion | flops 201326592 | bytes 1310720
  115.3 19.1 %all-gather.9.cloned.1.call-done = bf16[512,2048]{1,0:T(8,128)(2,1)} async-done(((bf16[512,512]{1,0:T(8,128)(2,1)}), bf16[512,2048]{1,0:T(8,128)(2,1)}) %all-gather.9.cloned.1.call-update) | async-done | bytes 2097168 | tf_op jit(solution)/shard_map/all_gather | solution.py:146
  134.4 4.3 %fusion.27 = bf16[512,512]{1,0:T(8,128)(2,1)} fusion(bf16[512,2048]{1,0:T(8,128)(2,1)} %all-gather.9.cloned.1.call-done, bf16[1,2048,512]{2,1,0:T(8,128)(2,1)} %param.33), kind=kOutput, calls=%fused_computation.47 | convolution fusion | flops 1074003968 | bytes 4718592 | tf_op jit(solution)/shard_map/dot_general | solution.py:145
  138.7 5.5 %all-to-all-start.1 = ((bf16[8,64,512]{2,1,0:T(8,128)(2,1)}), bf16[8,64,512]{2,1,0:T(8,128)(2,1)S(1)}, u32[]{:S(2)}, u32[]{:S(2)}) async-start(bf16[8,64,512]{2,1,0:T(8,128)(2,1)} %bitcast.19), calls=%async_computation.1 | async-start | bytes 1048576 | tf_op jit(solution)/shard_map/all_to_all | solution.py:151
  144.4 8.9 %all-gather.7.cloned.1.call-done = bf16[256,2048]{1,0:T(8,128)(2,1)} async-done(((bf16[256,512]{1,0:T(8,128)(2,1)}), bf16[256,2048]{1,0:T(8,128)(2,1)}) %all-gather.7.cloned.1.call-update) | async-done | bytes 1048592 | tf_op jit(solution)/shard_map/all_gather | solution.py:124
  153.3 3.3 %convolution_convert_fusion = bf16[256,512]{1,0:T(8,128)(2,1)} fusion(bf16[256,2048]{1,0:T(8,128)(2,1)} %all-gather.7.cloned.1.call-done, bf16[2048,512]{1,0:T(8,128)(2,1)} %param.25), kind=kOutput, calls=%fused_computation.49 | convolution fusion | flops 537001984 | bytes 3407872 | tf_op jit(solution)/shard_map/dot_general | solution.py:123
  156.7 2.4 %all-to-all-done.1 = bf16[8,64,512]{2,1,0:T(8,128)(2,1)S(1)} async-done(((bf16[8,64,512]{2,1,0:T(8,128)(2,1)}), bf16[8,64,512]{2,1,0:T(8,128)(2,1)S(1)}, u32[]{:S(2)}, u32[]{:S(2)}) %all-to-all-start.1) | async-done | bytes 524320 | tf_op jit(solution)/shard_map/all_to_all | solution.py:151
  160.6 1.4 multiply_reduce_fusion.1
  (119 shorter events, 34.6 us)
Async XLA Ops:
  7.2 66.2 %copy-start = (bf16[1,2048,512]{2,1,0:T(8,128)(2,1)S(1)}, bf16[1,2048,512]{2,1,0:T(8,128)(2,1)}, u32[]{:S(2)}) copy-start(bf16[1,2048,512]{2,1,0:T(8,128)(2,1)} %param.31) | copy-start | bytes 6291460
  17.6 7.5 %copy-start.5 = (f32[512]{0:T(512)S(1)}, f32[512]{0:T(512)}, u32[]{:S(2)}) copy-start(f32[512]{0:T(512)} %param.23) | copy-start | bytes 6148
  17.6 55.8 %all-to-all-start = ((bf16[8,64,2048]{2,1,0:T(8,128)(2,1)}), bf16[8,64,2048]{2,1,0:T(8,128)(2,1)}, u32[]{:S(2)}, u32[]{:S(2)}) async-start(bf16[8,64,2048]{2,1,0:T(8,128)(2,1)} %bitcast.133), calls=%async_computation | async-start | bytes 4194304 | tf_op jit(solution)/shard_map/all_to_all | solution.py:174
  25.0 86.6 %all-gather.11.cloned.1.call-start = ((), (), s32[]{:S(2)}) async-start(), calls=%async_computation.4 | async-start | bytes 1179648 | tf_op jit(solution)/shard_map/all_gather | solution.py:20
  69.8 64.7 %all-gather.9.cloned.1.call-start = ((), (), s32[]{:S(2)}) async-start(), calls=%async_computation.3 | async-start | bytes 2621440 | tf_op jit(solution)/shard_map/all_gather | solution.py:146
  73.3 3.0 %copy-start.7 = (bf16[1,2048,512]{2,1,0:T(8,128)(2,1)S(1)}, bf16[1,2048,512]{2,1,0:T(8,128)(2,1)}, u32[]{:S(2)}) copy-start(bf16[1,2048,512]{2,1,0:T(8,128)(2,1)} %param.32) | copy-start | bytes 6291460
  76.3 22.5 %copy-start.6 = (f32[128]{0:T(128)S(1)}, f32[128]{0:T(128)}, u32[]{:S(2)}) copy-start(f32[128]{0:T(128)} %param.24) | copy-start | bytes 1540
  80.1 73.2 %all-gather.7.cloned.1.call-start = ((), (), s32[]{:S(2)}) async-start(), calls=%async_computation.2 | async-start | bytes 1310720 | tf_op jit(solution)/shard_map/all_gather | solution.py:124
  111.6 1.7 %copy-start.1 = (f32[4,64,4,128]{3,1,0,2:T(8,128)S(1)}, f32[4,64,4,128]{3,1,0,2:T(8,128)}, u32[]{:S(2)}) copy-start(f32[4,64,4,128]{3,1,0,2:T(8,128)} %get-tuple-element.96) | copy-start | bytes 1572868
  111.6 2.8 %copy-start.2 = (bf16[256,512]{1,0:T(8,128)(2,1)S(1)}, bf16[256,512]{1,0:T(8,128)(2,1)}, u32[]{:S(2)}) copy-start(bf16[256,512]{1,0:T(8,128)(2,1)} %param.22) | copy-start | bytes 786436
  113.5 1.8 %copy-start.3 = (f32[128,4]{0,1:T(4,128)S(1)}, f32[128,4]{0,1:T(4,128)}, u32[]{:S(2)}) copy-start(f32[128,4]{0,1:T(4,128)} %param.29) | copy-start | bytes 6148
  115.3 28.9 %copy-start.4 = (f32[128,2]{0,1:T(2,128)S(1)}, f32[128,2]{0,1:T(2,128)}, u32[]{:S(2)}) copy-start(f32[128,2]{0,1:T(2,128)} %param.30) | copy-start | bytes 3076
  138.7 20.4 %all-to-all-start.1 = ((bf16[8,64,512]{2,1,0:T(8,128)(2,1)}), bf16[8,64,512]{2,1,0:T(8,128)(2,1)S(1)}, u32[]{:S(2)}, u32[]{:S(2)}) async-start(bf16[8,64,512]{2,1,0:T(8,128)(2,1)} %bitcast.19), calls=%async_computation.1 | async-start | bytes 1048576 | tf_op jit(solution)/shard_map/all_to_all | solution.py:151
Sparse Core Ops, SparseCore 0:
  69.9 41.6 all-gather.10
  113.1 21.2 all-gather.8
  136.6 16.7 all-gather.6
where the time goes:
time: 169 us; the launch traced here: 168 us
  waiting for transfers between devices  46.7 us (28%)
  other arithmetic  36.4 us (22%)
  matrix products  23.7 us (14%)
  blocking collectives  18.7 us (11%)
  local copies, waits for them, and re-layouts  15.7 us (9%)
  between operations  14 us (8%)
  starting transfers between devices  13 us (8%)
    all_gather x1, waiting for transfers between devices, finish(): lax.all_gather(hidden, 'tp', axis=1, tiled=True)  19.1 us
    all_gather x1, blocking collectives, entering(): lax.all_gather(a.astype(kind), axis)  18.7 us
    reduce_sum x4, other arithmetic, block_terms(): jnp.sum(query_block[:, None] * input_block[None, :] * decays, axis=-1)  14.9 us
    all_gather x1, waiting for transfers between devices, entering(): lax.all_gather(a.astype(kind), axis)  12.7 us
    all_gather x1, waiting for transfers between devices, mixer_local(): lax.all_gather(mixed_heads, 'tp', axis=1, tiled=True)  8.91 us
    all_to_all x1, starting transfers between devices, expert_local(): lax.all_to_all(outgoing, 'ep', split_axis=0, concat_axis=0, tiled=True)  7.41 us
    all_to_all x1, starting transfers between devices, finish(): return lax.all_to_all(shaped, 'ep', split_axis=0, concat_axis=0, tiled=True)  5.51 us
    dot_general x1, matrix products, finish(): jnp.dot(lax.all_gather(hidden, 'tp', axis=1, tiled=True), down_local, pre...  4.26 us
  transfers between devices with their start and end apart: 5, of which 5 were waited for; matrix products, arithmetic and copies ran while one was open for 37% of the time, Pallas kernels for 0%

commit v1 on v0

v1 whole, which is shorter than its diff:
```python
import jax
import jax.numpy as jnp
from jax import lax
from jax.experimental import pallas as pl
from jax.experimental.pallas import tpu as pltpu
from jax.sharding import PartitionSpec as P

KEYDIM = 128
VDIM = 128
GROUPS = 4
TOPK = 2
PAD = 8
norm_eps = 1e-06
F32 = jnp.float32
BF16 = jnp.bfloat16
VM = pl.BlockSpec(memory_space=pltpu.VMEM)
SM = pl.BlockSpec(memory_space=pltpu.SMEM)


def tn_dot(a, b):
    return lax.dot_general(a, b, (((0,), (0,)), ((), ())), preferred_element_type=F32)


def nt_dot(a, b):
    return lax.dot_general(a, b, (((1,), (1,)), ((), ())), preferred_element_type=F32)


def silu(v):
    return v / (1.0 + jnp.exp(-v))


def local_kernel(q_ref, f_ref, v_ref, floor_ref, intra_ref, qexp_ref, pay_ref):
    length = q_ref.shape[0]
    rows = lax.broadcasted_iota(jnp.int32, (length, length), 0)
    cols = lax.broadcasted_iota(jnp.int32, (length, length), 1)
    causal = cols <= rows
    tril = causal.astype(F32)
    for h in range(q_ref.shape[1] // KEYDIM):
        at = slice(h * KEYDIM, (h + 1) * KEYDIM)
        floor = floor_ref[:, at]
        rates = (1.0 - floor) / (1.0 + jnp.exp(f_ref[:, at].astype(F32)))
        cum = jnp.dot(
            tril, jnp.log(1.0 - rates), precision=lax.Precision.HIGHEST,
            preferred_element_type=F32,
        )
        end = cum[length - 1 : length, :]
        qexp = (silu(q_ref[:, at].astype(F32)) * jnp.exp(cum)).astype(BF16)
        kexp = (rates * jnp.exp(-cum)).astype(BF16)
        kend = (rates * jnp.exp(end - cum)).astype(BF16)
        value = v_ref[:, at]
        scores = jnp.where(causal, nt_dot(qexp, kexp), 0.0).astype(BF16)
        intra_ref[:, at] = jnp.dot(scores, value, preferred_element_type=F32)
        qexp_ref[:, at] = qexp
        pay_ref[h, :VDIM, :] = tn_dot(value, kend).astype(BF16)
        pay_ref[h, VDIM:, :] = jnp.broadcast_to(jnp.exp(end), (PAD, KEYDIM)).astype(BF16)


def finish_kernel(me_ref, all_ref, intra_ref, qexp_ref, gate_ref, gain_ref, out_ref):
    me = me_ref[0]
    for h in range(intra_ref.shape[1] // VDIM):
        at = slice(h * VDIM, (h + 1) * VDIM)

        def one(p, state):
            decay = all_ref[p, h, VDIM:, :].astype(F32)[:1]
            return state * decay + all_ref[p, h, :VDIM, :].astype(F32)

        state = lax.fori_loop(0, me, one, jnp.zeros((VDIM, KEYDIM), F32))
        out = intra_ref[:, at] + nt_dot(qexp_ref[:, at], state.astype(BF16))
        scale = lax.rsqrt(jnp.mean(out * out, axis=-1, keepdims=True) + norm_eps)
        out_ref[:, at] = (
            out * scale * gain_ref[...] * silu(gate_ref[:, at].astype(F32))
        ).astype(BF16)


def dispatch_kernel(half_ref, x_ref, gain_ref, routes_ref, gl_ref, cl_ref, out_ref, wt_ref):
    rows, width = x_ref.shape
    slots = out_ref.shape[0]
    part = out_ref.shape[1]
    experts = half_ref.shape[0] - 1
    capacity = slots // experts
    group_size = experts // GROUPS
    route = [routes_ref[:, j : j + 1] for j in range(TOPK)]
    ids = lax.broadcasted_iota(jnp.int32, (rows, experts), 1)
    hot = [(r == ids).astype(F32) for r in route]
    t0 = lax.broadcasted_iota(jnp.int32, (rows, rows), 0)
    t1 = lax.broadcasted_iota(jnp.int32, (rows, rows), 1)
    before = jnp.dot(
        (t1 < t0).astype(BF16), sum(hot).astype(BF16), preferred_element_type=F32
    )
    group_exp = jnp.exp(gl_ref[...])
    group_prob = group_exp / jnp.sum(group_exp, axis=-1, keepdims=True)
    gids = lax.broadcasted_iota(jnp.int32, (rows, GROUPS), 1)
    member = [
        ((r >= gids * group_size) & (r < (gids + 1) * group_size)).astype(F32) for r in route
    ]
    choice = [jnp.exp(cl_ref[:, j : j + 1]) for j in range(TOPK)]
    slot_ids = lax.broadcasted_iota(jnp.int32, (rows, slots), 1)
    place = jnp.zeros((rows, slots), F32)
    weight = jnp.zeros((rows, slots), F32)
    for j in range(TOPK):
        rank = jnp.sum(before * hot[j], axis=-1, keepdims=True).astype(jnp.int32)
        mark = (slot_ids == route[j] * capacity + rank).astype(F32)
        within = sum(
            jnp.sum(member[j] * member[i], axis=-1, keepdims=True) * choice[i]
            for i in range(TOPK)
        )
        prob = jnp.sum(member[j] * group_prob, axis=-1, keepdims=True)
        place = place + mark
        weight = weight + mark * (prob * choice[j] / within)
    high = weight.astype(BF16)
    wt_ref[0] = high
    wt_ref[1] = (weight - high.astype(F32)).astype(BF16)
    x = x_ref[...].astype(F32)
    scale = lax.rsqrt(jnp.mean(x * x, axis=-1, keepdims=True) + norm_eps)
    cols = pl.ds(pl.multiple_of(half_ref[0] * part, part), part)
    normed = (x_ref[:, cols].astype(F32) * scale * gain_ref[:, cols]).astype(BF16)
    out_ref[...] = tn_dot(place.astype(BF16), normed).astype(BF16)


def return_kernel(wt_ref, back_ref, out_ref):
    back = back_ref[...]
    out_ref[...] = (
        jnp.dot(wt_ref[0], back, preferred_element_type=F32)
        + jnp.dot(wt_ref[1], back, preferred_element_type=F32)
    ).astype(BF16)


def cost(flops, size):
    return pl.CostEstimate(flops=flops, bytes_accessed=size, transcendentals=0)


def shaped(shape, kind):
    return jax.ShapeDtypeStruct(shape, kind)


def per_device(
    mixer_query, mixer_forget, mixer_value, mixer_gate, forget_floor, head_gain, mixer_proj,
    expert_tokens, expert_gain, routes, group_logits, choice_logits, w_gate, w_up, w_down,
):
    length, width = mixer_query.shape
    heads = width // KEYDIM
    experts = lax.axis_size("ep")
    tp = lax.axis_size("tp")
    rows, model = expert_tokens.shape
    capacity = 2 * TOPK * rows // experts
    slots = experts * capacity
    split = 2
    part = model // split
    which = lax.axis_index("tp") % split
    half = jnp.full((experts + 1,), 0, jnp.int32) + which

    outgoing, wt = pl.pallas_call(
        dispatch_kernel,
        name="dispatch",
        out_shape=(shaped((slots, part), BF16), shaped((2, rows, slots), BF16)),
        in_specs=[SM, VM, VM, VM, VM, VM],
        out_specs=(VM, VM),
        cost_estimate=cost(2 * rows * slots * part, 4000000),
    )(half, expert_tokens, expert_gain[None, :], routes, group_logits, choice_logits)
    arrived = lax.all_to_all(
        outgoing.reshape(experts, capacity, part), "ep", split_axis=0, concat_axis=0, tiled=True
    )

    intra, qexp, pay = pl.pallas_call(
        local_kernel,
        name="local_scan",
        out_shape=(
            shaped((length, width), F32),
            shaped((length, width), BF16),
            shaped((heads, VDIM + PAD, KEYDIM), BF16),
        ),
        in_specs=[VM] * 4,
        out_specs=(VM, VM, VM),
        cost_estimate=cost(3000000000, 4000000),
    )(mixer_query, mixer_forget, mixer_value, forget_floor[None, :])
    everyone = lax.all_gather(pay, "ep")
    place = lax.axis_index("ep").astype(jnp.int32).reshape(1)
    mixed = pl.pallas_call(
        finish_kernel,
        name="mixer_finish",
        out_shape=shaped((length, width), BF16),
        in_specs=[SM] + [VM] * 5,
        out_specs=VM,
        cost_estimate=cost(1000000000, 4000000),
    )(place, everyone, intra, qexp, mixer_gate, head_gain[None, :])
    mixed_all = lax.all_gather(mixed, "tp", axis=1, tiled=True)

    groups = [list(range(s, s + split)) for s in range(0, tp, split)]
    flat_in = lax.all_gather(
        arrived.reshape(slots, part), "tp", axis=1, tiled=True, axis_index_groups=groups
    )
    gate_pre = jnp.dot(flat_in, w_gate[0], preferred_element_type=F32)
    up_pre = jnp.dot(flat_in, w_up[0], preferred_element_type=F32)
    hidden = (jax.nn.silu(gate_pre) * up_pre).astype(BF16)
    hidden_all = lax.all_gather(hidden, "tp", axis=1, tiled=True)
    mixer_out = jnp.dot(mixed_all, mixer_proj, preferred_element_type=F32).astype(BF16)
    down = jnp.dot(hidden_all, w_down[0], preferred_element_type=F32).astype(BF16)
    back = lax.all_to_all(
        down.reshape(experts, capacity, -1), "ep", split_axis=0, concat_axis=0, tiled=True
    ).reshape(slots, -1)
    expert_out = pl.pallas_call(
        return_kernel,
        name="weigh",
        out_shape=shaped((rows, back.shape[1]), BF16),
        in_specs=[VM, VM],
        out_specs=VM,
        cost_estimate=cost(4 * rows * slots * back.shape[1], 1000000),
    )(wt, back)
    return (mixer_out, expert_out)


def solution(mesh):
    return jax.shard_map(
        per_device,
        mesh=mesh,
        in_specs=(
            P("ep", "tp"),
            P("ep", "tp"),
            P("ep", "tp"),
            P("ep", "tp"),
            P("tp"),
            P(),
            P(None, "tp"),
            P("ep", None),
            P(),
            P("ep", None),
            P("ep", None),
            P("ep", None),
            P("ep", None, "tp"),
            P("ep", None, "tp"),
            P("ep", None, "tp"),
        ),
        out_specs=(P("ep", "tp"), P("ep", "tp")),
        check_vma=False,
    )
```

time: 169 us -> 159 us (0.941)
  other arithmetic: 36.4 us -> 0 us
  waiting for transfers between devices: 46.7 us -> 74.4 us
  blocking collectives: 18.7 us -> 33.1 us
  Pallas kernels: 0 us -> 13.6 us
  matrix products: 23.7 us -> 12.7 us
  local copies, waits for them, and re-layouts: 15.7 us -> 5.71 us
  starting transfers between devices: 13 us -> 5.67 us
    all_to_all x0 -> x1, blocking collectives: none -> 33.1 us  [per_device(): lax.all_to_all(outgoing.reshape(experts, capacity, part), 'ep', split_axi...]
    all_gather x3 -> x4, waiting for transfers between devices: 40.7 us -> 71.1 us  [the longest x1 39 us: per_device(): everyone = lax.all_gather(pay, 'ep')]
    all_gather x1 -> x0, blocking collectives: 18.7 us -> none  [entering(): lax.all_gather(a.astype(kind), axis)]
    reduce_sum x11 -> x0, other arithmetic: 17.9 us -> none  [the longest x4 14.9 us: block_terms(): jnp.sum(query_block[:, None] * input_block[None, :] * decays, axis=-1)]
    pallas_call x0 -> x4, Pallas kernels: none -> 13.6 us  [the longest x1 5.15 us: per_device(): pl.pallas_call(local_kernel, name='local_scan', out_shape=(shaped((length...]
    mul x10 -> x0, other arithmetic: 10.3 us -> none  [the longest x4 4.08 us: block_terms(): query_block * jnp.exp(cumulative_log)]
    dot_general x16 -> x4, matrix products: 22 us -> 12.7 us  [the longest x1 4.26 us: per_device(): jnp.dot(hidden_all, w_down[0], preferred_element_type=F32).astype(BF16)]
    all_to_all x2 -> x1, starting transfers between devices: 12.9 us -> 5.51 us  [per_device(): lax.all_to_all(down.reshape(experts, capacity, -1), 'ep', split_axis=0, c...]
  transfers between devices with their start and end apart: 5 -> 5, of which waited for: 5 -> 5; matrix products, arithmetic and copies ran while one was open for 37% -> 8% of each run, Pallas kernels for 0% -> 5%
where the time goes in v1:
time: 159 us
  waiting for transfers between devices  74.4 us (47%)
  blocking collectives  33.1 us (21%)
  between operations  13.8 us (9%)
  Pallas kernels  13.6 us (9%)
  matrix products  12.7 us (8%)
  local copies, waits for them, and re-layouts  5.71 us (4%)
  starting transfers between devices  5.67 us (4%)
    all_gather x1, waiting for transfers between devices, per_device(): everyone = lax.all_gather(pay, 'ep')  39 us
    all_to_all x1, blocking collectives, per_device(): lax.all_to_all(outgoing.reshape(experts, capacity, part), 'ep', split_axi...  33.1 us
    all_gather x1, waiting for transfers between devices, per_device(): hidden_all = lax.all_gather(hidden, 'tp', axis=1, tiled=True)  19.3 us
    all_gather x1, waiting for transfers between devices, per_device(): mixed_all = lax.all_gather(mixed, 'tp', axis=1, tiled=True)  8.37 us
    all_to_all x1, starting transfers between devices, per_device(): lax.all_to_all(down.reshape(experts, capacity, -1), 'ep', split_axis=0, c...  5.51 us
    unnamed x11, local copies, waits for them, and re-layouts  5.18 us
    pallas_call x1, Pallas kernels, per_device(): pl.pallas_call(local_kernel, name='local_scan', out_shape=(shaped((length...  5.15 us
    all_gather x1, waiting for transfers between devices, per_device(): lax.all_gather(arrived.reshape(slots, part), 'tp', axis=1, tiled=True, ax...  4.5 us
  transfers between devices with their start and end apart: 5, of which 5 were waited for; matrix products, arithmetic and copies ran while one was open for 8% of the time, Pallas kernels for 5%

profile of v1, /device:TPU:0, one launch (start us, length us, event | category | flops | bytes accessed | tf_op | source)
XLA Modules:
  0.0 159.0 jit_solution(15423940771370383585)
XLA Ops:
  7.2 0.0 all-gather.8.cloned.1.call-start
  7.2 1.6 copy.20.routes_ref
  8.8 1.4 copy.21.gl_ref
  10.2 1.4 copy.22.cl_ref
  11.6 0.5 add.12.half_ref
  12.1 3.1 %dispatch.1 = (bf16[512,1024]{1,0:T(8,128)(2,1)}, bf16[2,128,512]{2,1,0:T(8,128)(2,1)}) custom-call(s32[9]{0:T(128)} %add.12.half_ref, bf16[128,2048]{1,0:T(8,128)(2,1)} %x_ref.1, f32[1,2048]{1,0:T(1,128)} %bitcast.32, s32[128,2]{1,0:T(8,128)} %copy.20.routes_ref, f32[128,4]{1,0:T(8,128)} %copy.21.gl_ref, f32[128,2]{1,0:T(8,128)} %copy.22.cl_ref), custom_call_target="tpu_custom_call" | custom-call | flops 134217728 | bytes 4000000 | tf_op jit(solution)/shard_map/dispatch/pallas_call | solution.py:152
  15.2 33.1 %all_to_all.10 = bf16[8,64,1024]{2,1,0:T(8,128)(2,1)} all-to-all(bf16[8,64,1024]{2,1,0:T(8,128)(2,1)} %bitcast.31), channel_id=1, replica_groups=mesh['ep'=8,'tp'=4] {'ep'}, dimensions={0} | all-to-all | bytes 2097152 | tf_op jit(solution)/shard_map/all_to_all | solution.py:160
  48.4 0.0 all-gather.12.cloned.1.call-start
  48.5 5.1 %local_scan.1 = (f32[256,512]{1,0:T(8,128)}, bf16[256,512]{1,0:T(8,128)(2,1)}, bf16[4,136,128]{2,1,0:T(8,128)(2,1)}) custom-call(bf16[256,512]{1,0:T(8,128)(2,1)} %q_ref.1, bf16[256,512]{1,0:T(8,128)(2,1)} %f_ref.1, bf16[256,512]{1,0:T(8,128)(2,1)} %v_ref.1, f32[1,512]{1,0:T(1,128)} %bitcast.34), custom_call_target="tpu_custom_call" | custom-call | flops 3000000000 | bytes 4000000 | tf_op jit(solution)/shard_map/local_scan/pallas_call | solution.py:164
  53.6 0.0 all-gather.10.cloned.1.call-start
  53.7 4.5 %all-gather.8.cloned.1.call-done = bf16[512,2048]{1,0:T(8,128)(2,1)} async-done(((bf16[512,1024]{1,0:T(8,128)(2,1)}), bf16[512,2048]{1,0:T(8,128)(2,1)}) %all-gather.8.cloned.1.call-update) | async-done | bytes 2097168 | tf_op jit(solution)/shard_map/all_gather | solution.py:189
  58.2 3.0 %fusion.4 = f32[512,512]{1,0:T(8,128)S(1)} fusion(bf16[512,2048]{1,0:T(8,128)(2,1)} %all-gather.8.cloned.1.call-done, bf16[1,2048,512]{2,1,0:T(8,128)(2,1)S(1)} %copy-done), kind=kOutput, calls=%fused_computation.4 | convolution fusion | flops 1073741824 | bytes 5242880 | tf_op jit(solution)/shard_map/dot_general | solution.py:192
  61.2 2.1 %fusion.12 = bf16[512,512]{1,0:T(8,128)(2,1)} fusion(bf16[512,2048]{1,0:T(8,128)(2,1)S(1)} %copy-done.3, bf16[1,2048,512]{2,1,0:T(8,128)(2,1)S(1)} %copy-done.2, f32[512,512]{1,0:T(8,128)S(1)} %fusion.4), kind=kOutput, calls=%fused_computation.8 | convolution fusion | flops 1075314688 | bytes 5767168 | tf_op jit(solution)/shard_map/dot_general | solution.py:193
  63.3 0.0 all-gather.6.cloned.1.call-start
  63.4 39.0 %all-gather.12.cloned.1.call-done = bf16[32,136,128]{2,1,0:T(8,128)(2,1)} async-done(((bf16[4,136,128]{2,1,0:T(8,128)(2,1)}), bf16[32,136,128]{2,1,0:T(8,128)(2,1)}) %all-gather.12.cloned.1.call-update) | async-done | bytes 1114128 | tf_op jit(solution)/shard_map/all_gather | solution.py:176
  102.3 3.3 %mixer_finish.1 = bf16[256,512]{1,0:T(8,128)(2,1)} custom-call(s32[1]{0:T(128)} %bitcast.me_ref, bf16[8,4,136,128]{3,2,1,0:T(8,128)(2,1)} %bitcast.33, f32[256,512]{1,0:T(8,128)} %get-tuple-element.8.intra_ref, bf16[256,512]{1,0:T(8,128)(2,1)} %get-tuple-element.9.qexp_ref, bf16[256,512]{1,0:T(8,128)(2,1)} %gate_ref.1, f32[1,128]{1,0:T(1,128)} %bitcast.35), custom_call_target="tpu_custom_call" | custom-call | flops 1000000000 | bytes 4000000 | tf_op jit(solution)/shard_map/mixer_finish/pallas_call | solution.py:178
  105.7 19.3 %all-gather.10.cloned.1.call-done = bf16[512,2048]{1,0:T(8,128)(2,1)} async-done(((bf16[512,512]{1,0:T(8,128)(2,1)}), bf16[512,2048]{1,0:T(8,128)(2,1)}) %all-gather.10.cloned.1.call-update) | async-done | bytes 2097168 | tf_op jit(solution)/shard_map/all_gather | solution.py:195
  125.0 4.3 %fusion.9 = bf16[512,512]{1,0:T(8,128)(2,1)} fusion(bf16[512,2048]{1,0:T(8,128)(2,1)} %all-gather.10.cloned.1.call-done, bf16[1,2048,512]{2,1,0:T(8,128)(2,1)} %param.29), kind=kOutput, calls=%fused_computation.7 | convolution fusion | flops 1074003968 | bytes 4718592 | tf_op jit(solution)/shard_map/dot_general | solution.py:197
  129.2 5.5 %all-to-all-start.1 = ((bf16[8,64,512]{2,1,0:T(8,128)(2,1)}), bf16[8,64,512]{2,1,0:T(8,128)(2,1)S(1)}, u32[]{:S(2)}, u32[]{:S(2)}) async-start(bf16[8,64,512]{2,1,0:T(8,128)(2,1)} %bitcast.10), calls=%async_computation.1 | async-start | bytes 1048576 | tf_op jit(solution)/shard_map/all_to_all | solution.py:198
  134.7 8.4 %all-gather.6.cloned.1.call-done = bf16[256,2048]{1,0:T(8,128)(2,1)} async-done(((bf16[256,512]{1,0:T(8,128)(2,1)}), bf16[256,2048]{1,0:T(8,128)(2,1)}) %all-gather.6.cloned.1.call-update) | async-done | bytes 1048592 | tf_op jit(solution)/shard_map/all_gather | solution.py:186
  143.1 3.3 %convolution_convert_fusion = bf16[256,512]{1,0:T(8,128)(2,1)} fusion(bf16[256,2048]{1,0:T(8,128)(2,1)} %all-gather.6.cloned.1.call-done, bf16[2048,512]{1,0:T(8,128)(2,1)} %param.21), kind=kOutput, calls=%fused_computation.9 | convolution fusion | flops 537001984 | bytes 3407872 | tf_op jit(solution)/shard_map/dot_general | solution.py:196
  146.4 3.2 %all-to-all-done.1 = bf16[8,64,512]{2,1,0:T(8,128)(2,1)S(1)} async-done(((bf16[8,64,512]{2,1,0:T(8,128)(2,1)}), bf16[8,64,512]{2,1,0:T(8,128)(2,1)S(1)}, u32[]{:S(2)}, u32[]{:S(2)}) %all-to-all-start.1) | async-done | bytes 524320 | tf_op jit(solution)/shard_map/all_to_all | solution.py:198
  149.6 0.8 copy-done.1
  150.4 2.1 %weigh.1 = bf16[128,512]{1,0:T(8,128)(2,1)} custom-call(bf16[2,128,512]{2,1,0:T(8,128)(2,1)} %get-tuple-element.10.wt_ref, bf16[512,512]{1,0:T(8,128)(2,1)} %bitcast.30), custom_call_target="tpu_custom_call" | custom-call | flops 134217728 | bytes 1000000 | tf_op jit(solution)/shard_map/weigh/pallas_call | solution.py:201
  (11 shorter events, 0.1 us)
Async XLA Ops:
  7.2 51.0 %copy-start = (bf16[1,2048,512]{2,1,0:T(8,128)(2,1)S(1)}, bf16[1,2048,512]{2,1,0:T(8,128)(2,1)}, u32[]{:S(2)}) copy-start(bf16[1,2048,512]{2,1,0:T(8,128)(2,1)} %param.27) | copy-start | bytes 6291460
  7.2 51.0 %all-gather.8.cloned.1.call-start = ((), (), s32[]{:S(2)}) async-start(), calls=%async_computation.3 | async-start | bytes 3145728 | tf_op jit(solution)/shard_map/all_gather | solution.py:189
  48.4 53.9 %all-gather.12.cloned.1.call-start = ((), (), s32[]{:S(2)}) async-start(), calls=%async_computation.5 | async-start | bytes 1253376 | tf_op jit(solution)/shard_map/all_gather | solution.py:176
  53.6 71.3 %all-gather.10.cloned.1.call-start = ((), (), s32[]{:S(2)}) async-start(), calls=%async_computation.4 | async-start | bytes 2621440 | tf_op jit(solution)/shard_map/all_gather | solution.py:195
  58.2 3.0 %copy-start.2 = (bf16[1,2048,512]{2,1,0:T(8,128)(2,1)S(1)}, bf16[1,2048,512]{2,1,0:T(8,128)(2,1)}, u32[]{:S(2)}) copy-start(bf16[1,2048,512]{2,1,0:T(8,128)(2,1)} %param.28) | copy-start | bytes 6291460
  58.2 3.0 %copy-start.3 = (bf16[512,2048]{1,0:T(8,128)(2,1)S(1)}, bf16[512,2048]{1,0:T(8,128)(2,1)}, u32[]{:S(2)}) copy-start(bf16[512,2048]{1,0:T(8,128)(2,1)} %all-gather.8.cloned.1.call-done) | copy-start | bytes 6291460
  63.3 79.8 %all-gather.6.cloned.1.call-start = ((), (), s32[]{:S(2)}) async-start(), calls=%async_computation.2 | async-start | bytes 1310720 | tf_op jit(solution)/shard_map/all_gather | solution.py:186
  129.2 20.4 %all-to-all-start.1 = ((bf16[8,64,512]{2,1,0:T(8,128)(2,1)}), bf16[8,64,512]{2,1,0:T(8,128)(2,1)S(1)}, u32[]{:S(2)}, u32[]{:S(2)}) async-start(bf16[8,64,512]{2,1,0:T(8,128)(2,1)} %bitcast.10), calls=%async_computation.1 | async-start | bytes 1048576 | tf_op jit(solution)/shard_map/all_to_all | solution.py:198
  149.6 0.8 copy-start.1
Sparse Core Ops, SparseCore 0:
  48.5 9.5 all-gather.7
  60.4 41.9 all-gather.11
  103.9 21.0 all-gather.9
  126.4 16.6 all-gather.5

commit v2 on v1

--- a/solution.py
+++ b/solution.py
@@ -55,17 +55,11 @@
         pay_ref[h, VDIM:, :] = jnp.broadcast_to(jnp.exp(end), (PAD, KEYDIM)).astype(BF16)
 
 
-def finish_kernel(me_ref, all_ref, intra_ref, qexp_ref, gate_ref, gain_ref, out_ref):
-    me = me_ref[0]
+def finish_kernel(state_ref, intra_ref, qexp_ref, gate_ref, gain_ref, out_ref):
     for h in range(intra_ref.shape[1] // VDIM):
         at = slice(h * VDIM, (h + 1) * VDIM)
 
-        def one(p, state):
-            decay = all_ref[p, h, VDIM:, :].astype(F32)[:1]
-            return state * decay + all_ref[p, h, :VDIM, :].astype(F32)
-
-        state = lax.fori_loop(0, me, one, jnp.zeros((VDIM, KEYDIM), F32))
-        out = intra_ref[:, at] + nt_dot(qexp_ref[:, at], state.astype(BF16))
+        out = intra_ref[:, at] + nt_dot(qexp_ref[:, at], state_ref[h, :VDIM, :])
         scale = lax.rsqrt(jnp.mean(out * out, axis=-1, keepdims=True) + norm_eps)
         out_ref[:, at] = (
             out * scale * gain_ref[...] * silu(gate_ref[:, at].astype(F32))
@@ -125,6 +119,26 @@
     ).astype(BF16)
 
 
+def later_after(later, earlier):
+    later = later.astype(F32)
+    rows = lax.broadcasted_iota(jnp.int32, later.shape, 1)
+    decay = later[:, VDIM : VDIM + 1, :]
+    return (decay * earlier.astype(F32) + jnp.where(rows < VDIM, later, 0.0)).astype(BF16)
+
+
+def prefix(pay, count):
+    span = pay
+    before = None
+    step = 1
+    while step < count:
+        came = lax.ppermute(span, "ep", [(i, i + step) for i in range(count - step)])
+        before = came if before is None else later_after(before, came)
+        step *= 2
+        if step < count:
+            span = later_after(span, came)
+    return jnp.zeros_like(pay) if before is None else before
+
+
 def cost(flops, size):
     return pl.CostEstimate(flops=flops, bytes_accessed=size, transcendentals=0)
 
@@ -173,21 +187,22 @@
         out_specs=(VM, VM, VM),
         cost_estimate=cost(3000000000, 4000000),
     )(mixer_query, mixer_forget, mixer_value, forget_floor[None, :])
-    everyone = lax.all_gather(pay, "ep")
-    place = lax.axis_index("ep").astype(jnp.int32).reshape(1)
+    entering = prefix(pay, experts)
     mixed = pl.pallas_call(
         finish_kernel,
         name="mixer_finish",
         out_shape=shaped((length, width), BF16),
-        in_specs=[SM] + [VM] * 5,
+        in_specs=[VM] * 5,
         out_specs=VM,
         cost_estimate=cost(1000000000, 4000000),
-    )(place, everyone, intra, qexp, mixer_gate, head_gain[None, :])
+    )(entering, intra, qexp, mixer_gate, head_gain[None, :])
+
+    arrived, mixed = lax.optimization_barrier((arrived, mixed))
     mixed_all = lax.all_gather(mixed, "tp", axis=1, tiled=True)
-
-    groups = [list(range(s, s + split)) for s in range(0, tp, split)]
-    flat_in = lax.all_gather(
-        arrived.reshape(slots, part), "tp", axis=1, tiled=True, axis_index_groups=groups
+    own = arrived.reshape(slots, part)
+    other = lax.ppermute(own, "tp", [(i, i ^ 1) for i in range(tp)])
+    flat_in = jnp.concatenate(
+        [jnp.where(which == 0, own, other), jnp.where(which == 0, other, own)], axis=1
     )
     gate_pre = jnp.dot(flat_in, w_gate[0], preferred_element_type=F32)
     up_pre = jnp.dot(flat_in, w_up[0], preferred_element_type=F32)

time: 159 us -> 137 us (0.86)
  starting transfers between devices: 5.67 us -> 40.1 us
  blocking collectives: 33.1 us -> 0 us
  waiting for transfers between devices: 74.4 us -> 48.7 us
  other arithmetic: 0 us -> 3.29 us
  matrix products: 12.7 us -> 11 us
    all_gather x2 -> x0, waiting for transfers between devices: 43.4 us -> none  [the longest x1 39 us: per_device(): everyone = lax.all_gather(pay, 'ep')]
    all_to_all x1 -> x0, blocking collectives: 33.1 us -> none  [per_device(): lax.all_to_all(outgoing.reshape(experts, capacity, part), 'ep', split_axi...]
    ppermute x0 -> x4, starting transfers between devices: none -> 27.3 us  [the longest x3 27.3 us: prefix(): lax.ppermute(span, 'ep', [(i, i + step) for i in range(count - step)])]
    ppermute x0 -> x4, waiting for transfers between devices: none -> 11.8 us  [the longest x3 8.97 us: prefix(): lax.ppermute(span, 'ep', [(i, i + step) for i in range(count - step)])]
    all_to_all x0 -> x1, starting transfers between devices: none -> 7.27 us  [per_device(): lax.all_to_all(outgoing.reshape(experts, capacity, part), 'ep', split_axi...]
    all_gather x1, waiting for transfers between devices: 19.3 us -> 24.7 us  [per_device(): hidden_all = lax.all_gather(hidden, 'tp', axis=1, tiled=True)]
    convert_element_type x0 -> x3, other arithmetic: none -> 1.92 us  [later_after(): (decay * earlier.astype(F32) + jnp.where(rows < VDIM, later, 0.0)).astype...]
    dot_general x1, matrix products: 2.98 us -> 1.24 us  [per_device(): gate_pre = jnp.dot(flat_in, w_gate[0], preferred_element_type=F32)]
  transfers between devices with their start and end apart: 5 -> 8, of which waited for: 5 -> 7; matrix products, arithmetic and copies ran while one was open for 8% -> 7% of each run, Pallas kernels for 5% -> 6%
where the time goes in v2:
time: 137 us
  waiting for transfers between devices  48.7 us (36%)
  starting transfers between devices  40.1 us (29%)
  between operations  14.1 us (10%)
  Pallas kernels  12.7 us (9%)
  matrix products  11 us (8%)
  local copies, waits for them, and re-layouts  6.81 us (5%)
  other arithmetic  3.29 us (2%)
    ppermute x3, starting transfers between devices, prefix(): lax.ppermute(span, 'ep', [(i, i + step) for i in range(count - step)])  27.3 us
    all_gather x1, waiting for transfers between devices, per_device(): hidden_all = lax.all_gather(hidden, 'tp', axis=1, tiled=True)  24.7 us
    ppermute x3, waiting for transfers between devices, prefix(): lax.ppermute(span, 'ep', [(i, i + step) for i in range(count - step)])  8.97 us
    all_gather x1, waiting for transfers between devices, per_device(): mixed_all = lax.all_gather(mixed, 'tp', axis=1, tiled=True)  8.51 us
    all_to_all x1, starting transfers between devices, per_device(): lax.all_to_all(outgoing.reshape(experts, capacity, part), 'ep', split_axi...  7.27 us
    unnamed x9, local copies, waits for them, and re-layouts  5.52 us
    all_to_all x1, starting transfers between devices, per_device(): lax.all_to_all(down.reshape(experts, capacity, -1), 'ep', split_axis=0, c...  5.51 us
    pallas_call x1, Pallas kernels, per_device(): pl.pallas_call(local_kernel, name='local_scan', out_shape=(shaped((length...  5.14 us
  transfers between devices with their start and end apart: 8, of which 7 were waited for; matrix products, arithmetic and copies ran while one was open for 7% of the time, Pallas kernels for 6%

profile of v2, /device:TPU:0, one launch (start us, length us, event | category | flops | bytes accessed | tf_op | source)
XLA Modules:
  0.0 136.8 jit_solution(15128698728444933939)
XLA Ops:
  7.2 1.6 %copy.17.routes_ref = s32[128,2]{1,0:T(8,128)} copy(s32[128,2]{0,1:T(2,128)} %param.24) | data formatting | bytes 2048 | tf_op args[9]
  8.7 1.4 %copy.18.gl_ref = f32[128,4]{1,0:T(8,128)} copy(f32[128,4]{0,1:T(4,128)} %param.25) | data formatting | bytes 4096 | tf_op args[10]
  10.2 1.4 %copy.19.cl_ref = f32[128,2]{1,0:T(8,128)} copy(f32[128,2]{0,1:T(2,128)} %param.26) | data formatting | bytes 2048 | tf_op args[11]
  12.1 3.1 %dispatch.1 = (bf16[512,1024]{1,0:T(8,128)(2,1)}, bf16[2,128,512]{2,1,0:T(8,128)(2,1)}) custom-call(s32[9]{0:T(128)} %add.24.half_ref, bf16[128,2048]{1,0:T(8,128)(2,1)} %x_ref.1, f32[1,2048]{1,0:T(1,128)} %bitcast.32, s32[128,2]{1,0:T(8,128)} %copy.17.routes_ref, f32[128,4]{1,0:T(8,128)} %copy.18.gl_ref, f32[128,2]{1,0:T(8,128)} %copy.19.cl_ref), custom_call_target="tpu_custom_call" | custom-call | flops 134217728 | bytes 4000000 | tf_op jit(solution)/shard_map/dispatch/pallas_call | solution.py:166
  15.2 7.3 %all-to-all-start = ((bf16[8,64,1024]{2,1,0:T(8,128)(2,1)}), bf16[8,64,1024]{2,1,0:T(8,128)(2,1)S(1)}, u32[]{:S(2)}, u32[]{:S(2)}) async-start(bf16[8,64,1024]{2,1,0:T(8,128)(2,1)} %bitcast.31), calls=%async_computation | async-start | bytes 2097152 | tf_op jit(solution)/shard_map/all_to_all | solution.py:174
  22.6 5.1 %local_scan.1 = (f32[256,512]{1,0:T(8,128)}, bf16[256,512]{1,0:T(8,128)(2,1)}, bf16[4,136,128]{2,1,0:T(8,128)(2,1)}) custom-call(bf16[256,512]{1,0:T(8,128)(2,1)} %q_ref.1, bf16[256,512]{1,0:T(8,128)(2,1)} %f_ref.1, bf16[256,512]{1,0:T(8,128)(2,1)} %v_ref.1, f32[1,512]{1,0:T(1,128)} %bitcast.37), custom_call_target="tpu_custom_call" | custom-call | flops 3000000000 | bytes 4000000 | tf_op jit(solution)/shard_map/local_scan/pallas_call | solution.py:178
  27.7 3.9 %collective-permute-start = (bf16[4,136,128]{2,1,0:T(8,128)(2,1)}, bf16[4,136,128]{2,1,0:T(8,128)(2,1)S(1)}, u32[]{:S(2)}, u32[]{:S(2)}) collective-permute-start(bf16[4,136,128]{2,1,0:T(8,128)(2,1)} %get-tuple-element.10), channel_id=1, source_target_pairs={{0,4},{4,8},{8,12},{12,16},{16,20},{20,24},{24,28},{1,5},{5,9},{9,... | collective-permute-start | bytes 417800 | tf_op jit(solution)/shard_map/ppermute | solution.py:134
  32.3 3.9 %collective-permute-done = bf16[4,136,128]{2,1,0:T(8,128)(2,1)S(1)} collective-permute-done((bf16[4,136,128]{2,1,0:T(8,128)(2,1)}, bf16[4,136,128]{2,1,0:T(8,128)(2,1)S(1)}, u32[]{:S(2)}, u32[]{:S(2)}) %collective-permute-start) | collective-permute-done | bytes 139296 | tf_op jit(solution)/shard_map/ppermute | solution.py:134
  37.2 13.0 %collective-permute-start.1 = (bf16[4,136,128]{2,1,0:T(8,128)(2,1)S(1)}, bf16[4,136,128]{2,1,0:T(8,128)(2,1)S(1)}, u32[]{:S(2)}, u32[]{:S(2)}) collective-permute-start(bf16[4,136,128]{2,1,0:T(8,128)(2,1)S(1)} %add_convert_fusion.1), channel_id=1, source_target_pairs={{0,8},{4,12},{8,16},{12,20},{16,24},{20,28},{1,9},{5,13},{9,17},{1... | collective-permute-start | bytes 417800 | tf_op jit(solution)/shard_map/ppermute | solution.py:134
  50.2 2.5 %collective-permute-done.1 = bf16[4,136,128]{2,1,0:T(8,128)(2,1)S(1)} collective-permute-done((bf16[4,136,128]{2,1,0:T(8,128)(2,1)S(1)}, bf16[4,136,128]{2,1,0:T(8,128)(2,1)S(1)}, u32[]{:S(2)}, u32[]{:S(2)}) %collective-permute-start.1) | collective-permute-done | bytes 139296 | tf_op jit(solution)/shard_map/ppermute | solution.py:134
  52.9 10.4 %collective-permute-start.2 = (bf16[4,136,128]{2,1,0:T(8,128)(2,1)S(1)}, bf16[4,136,128]{2,1,0:T(8,128)(2,1)S(1)}, u32[]{:S(2)}, u32[]{:S(2)}) collective-permute-start(bf16[4,136,128]{2,1,0:T(8,128)(2,1)S(1)} %get-tuple-element.18), channel_id=1, source_target_pairs={{0,16},{4,20},{8,24},{12,28},{1,17},{5,21},{9,25},{13,29},{2,18},{... | collective-permute-start | bytes 417800 | tf_op jit(solution)/shard_map/ppermute | solution.py:134
  63.3 2.6 %collective-permute-done.2 = bf16[4,136,128]{2,1,0:T(8,128)(2,1)S(1)} collective-permute-done((bf16[4,136,128]{2,1,0:T(8,128)(2,1)S(1)}, bf16[4,136,128]{2,1,0:T(8,128)(2,1)S(1)}, u32[]{:S(2)}, u32[]{:S(2)}) %collective-permute-start.2) | collective-permute-done | bytes 139296 | tf_op jit(solution)/shard_map/ppermute | solution.py:134
  66.7 2.4 %mixer_finish.1 = bf16[256,512]{1,0:T(8,128)(2,1)} custom-call(bf16[4,136,128]{2,1,0:T(8,128)(2,1)} %add_convert_fusion.state_ref, f32[256,512]{1,0:T(8,128)} %get-tuple-element.11.intra_ref, bf16[256,512]{1,0:T(8,128)(2,1)} %get-tuple-element.12.qexp_ref, bf16[256,512]{1,0:T(8,128)(2,1)} %gate_ref.1, f32[1,128]{1,0:T(1,128)} %bitcast.38), custom_call_target="tpu_custom_call" | custom-call | flops 1000000000 | bytes 4000000 | tf_op jit(solution)/shard_map/mixer_finish/pallas_call | solution.py:191
  69.0 2.8 %collective-permute-done.3 = bf16[512,1024]{1,0:T(8,128)(2,1)} collective-permute-done((bf16[512,1024]{1,0:T(8,128)(2,1)S(1)}, bf16[512,1024]{1,0:T(8,128)(2,1)}, u32[]{:S(2)}, u32[]{:S(2)}) %collective-permute-start.3) | collective-permute-done | bytes 1048608 | tf_op jit(solution)/shard_map/ppermute | solution.py:203
  71.8 1.4 broadcast_select_fusion.1
  73.2 1.2 fusion.4
  74.8 2.1 %multiply_convert_fusion = bf16[512,512]{1,0:T(8,128)(2,1)} fusion(f32[512,512]{1,0:T(8,128)S(1)} %fusion.4, bf16[1,2048,512]{2,1,0:T(8,128)(2,1)S(1)} %copy-done.2, bf16[512,1024]{1,0:T(8,128)(2,1)S(1)} %get-tuple-element.17, bf16[512,1024]{1,0:T(8,128)(2,1)S(1)} %get-tuple-element.16), kind=kOutput, calls=%fused_computation.9 | convolution fusion | flops 1079508992 | bytes 5767168 | tf_op jit(solution)/shard_map/dot_general | solution.py:208
  77.7 24.7 %all-gather.5.cloned.1.call-done = bf16[512,2048]{1,0:T(8,128)(2,1)} async-done(((bf16[512,512]{1,0:T(8,128)(2,1)}), bf16[512,2048]{1,0:T(8,128)(2,1)}) %all-gather.5.cloned.1.call-update) | async-done | bytes 2097168 | tf_op jit(solution)/shard_map/all_gather | solution.py:210
  102.4 4.3 %fusion.6 = bf16[512,512]{1,0:T(8,128)(2,1)} fusion(bf16[512,2048]{1,0:T(8,128)(2,1)} %all-gather.5.cloned.1.call-done, bf16[1,2048,512]{2,1,0:T(8,128)(2,1)} %param.29), kind=kOutput, calls=%fused_computation.7 | convolution fusion | flops 1074003968 | bytes 4718592 | tf_op jit(solution)/shard_map/dot_general | solution.py:212
  106.7 5.5 %all-to-all-start.1 = ((bf16[8,64,512]{2,1,0:T(8,128)(2,1)}), bf16[8,64,512]{2,1,0:T(8,128)(2,1)S(1)}, u32[]{:S(2)}, u32[]{:S(2)}) async-start(bf16[8,64,512]{2,1,0:T(8,128)(2,1)} %bitcast.12), calls=%async_computation.1 | async-start | bytes 1048576 | tf_op jit(solution)/shard_map/all_to_all | solution.py:213
  112.2 8.5 %all-gather.3.cloned.1.call-done = bf16[256,2048]{1,0:T(8,128)(2,1)} async-done(((bf16[256,512]{1,0:T(8,128)(2,1)}), bf16[256,2048]{1,0:T(8,128)(2,1)}) %all-gather.3.cloned.1.call-update) | async-done | bytes 1048592 | tf_op jit(solution)/shard_map/all_gather | solution.py:201
  120.7 3.3 %convolution_convert_fusion = bf16[256,512]{1,0:T(8,128)(2,1)} fusion(bf16[256,2048]{1,0:T(8,128)(2,1)} %all-gather.3.cloned.1.call-done, bf16[2048,512]{1,0:T(8,128)(2,1)} %param.21), kind=kOutput, calls=%fused_computation.8 | convolution fusion | flops 537001984 | bytes 3407872 | tf_op jit(solution)/shard_map/dot_general | solution.py:211
  124.1 3.0 %all-to-all-done.1 = bf16[8,64,512]{2,1,0:T(8,128)(2,1)S(1)} async-done(((bf16[8,64,512]{2,1,0:T(8,128)(2,1)}), bf16[8,64,512]{2,1,0:T(8,128)(2,1)S(1)}, u32[]{:S(2)}, u32[]{:S(2)}) %all-to-all-start.1) | async-done | bytes 524320 | tf_op jit(solution)/shard_map/all_to_all | solution.py:213
  127.9 2.1 %weigh.1 = bf16[128,512]{1,0:T(8,128)(2,1)} custom-call(bf16[2,128,512]{2,1,0:T(8,128)(2,1)} %get-tuple-element.14.wt_ref, bf16[512,512]{1,0:T(8,128)(2,1)} %bitcast.30), custom_call_target="tpu_custom_call" | custom-call | flops 134217728 | bytes 1000000 | tf_op jit(solution)/shard_map/weigh/pallas_call | solution.py:216
  (21 shorter events, 5.2 us)
Async XLA Ops:
  7.2 66.0 %copy-start = (bf16[1,2048,512]{2,1,0:T(8,128)(2,1)S(1)}, bf16[1,2048,512]{2,1,0:T(8,128)(2,1)}, u32[]{:S(2)}) copy-start(bf16[1,2048,512]{2,1,0:T(8,128)(2,1)} %param.27) | copy-start | bytes 6291460
  15.2 53.8 %all-to-all-start = ((bf16[8,64,1024]{2,1,0:T(8,128)(2,1)}), bf16[8,64,1024]{2,1,0:T(8,128)(2,1)S(1)}, u32[]{:S(2)}, u32[]{:S(2)}) async-start(bf16[8,64,1024]{2,1,0:T(8,128)(2,1)} %bitcast.31), calls=%async_computation | async-start | bytes 2097152 | tf_op jit(solution)/shard_map/all_to_all | solution.py:174
  22.5 79.9 %all-gather.5.cloned.1.call-start = ((), (), s32[]{:S(2)}) async-start(), calls=%async_computation.3 | async-start | bytes 2621440 | tf_op jit(solution)/shard_map/all_gather | solution.py:210
  27.7 8.5 %collective-permute-start = (bf16[4,136,128]{2,1,0:T(8,128)(2,1)}, bf16[4,136,128]{2,1,0:T(8,128)(2,1)S(1)}, u32[]{:S(2)}, u32[]{:S(2)}) collective-permute-start(bf16[4,136,128]{2,1,0:T(8,128)(2,1)} %get-tuple-element.10), channel_id=1, source_target_pairs={{0,4},{4,8},{8,12},{12,16},{16,20},{20,24},{24,28},{1,5},{5,9},{9,... | collective-permute-start | bytes 417800 | tf_op jit(solution)/shard_map/ppermute | solution.py:134
  37.2 15.6 %collective-permute-start.1 = (bf16[4,136,128]{2,1,0:T(8,128)(2,1)S(1)}, bf16[4,136,128]{2,1,0:T(8,128)(2,1)S(1)}, u32[]{:S(2)}, u32[]{:S(2)}) collective-permute-start(bf16[4,136,128]{2,1,0:T(8,128)(2,1)S(1)} %add_convert_fusion.1), channel_id=1, source_target_pairs={{0,8},{4,12},{8,16},{12,20},{16,24},{20,28},{1,9},{5,13},{9,17},{1... | collective-permute-start | bytes 417800 | tf_op jit(solution)/shard_map/ppermute | solution.py:134
  52.9 12.9 %collective-permute-start.2 = (bf16[4,136,128]{2,1,0:T(8,128)(2,1)S(1)}, bf16[4,136,128]{2,1,0:T(8,128)(2,1)S(1)}, u32[]{:S(2)}, u32[]{:S(2)}) collective-permute-start(bf16[4,136,128]{2,1,0:T(8,128)(2,1)S(1)} %get-tuple-element.18), channel_id=1, source_target_pairs={{0,16},{4,20},{8,24},{12,28},{1,17},{5,21},{9,25},{13,29},{2,18},{... | collective-permute-start | bytes 417800 | tf_op jit(solution)/shard_map/ppermute | solution.py:134
  69.0 2.8 %collective-permute-start.3 = (bf16[512,1024]{1,0:T(8,128)(2,1)S(1)}, bf16[512,1024]{1,0:T(8,128)(2,1)}, u32[]{:S(2)}, u32[]{:S(2)}) collective-permute-start(bf16[512,1024]{1,0:T(8,128)(2,1)S(1)} %bitcast.29), channel_id=1, source_target_pairs={{0,1},{1,0},{2,3},{3,2},{4,5},{5,4},{6,7},{7,6},{8,9},{9,8},{10,11... | collective-permute-start | bytes 3145736 | tf_op jit(solution)/shard_map/ppermute | solution.py:203
  73.2 1.6 %copy-start.2 = (bf16[1,2048,512]{2,1,0:T(8,128)(2,1)S(1)}, bf16[1,2048,512]{2,1,0:T(8,128)(2,1)}, u32[]{:S(2)}) copy-start(bf16[1,2048,512]{2,1,0:T(8,128)(2,1)} %param.28) | copy-start | bytes 6291460
  77.0 43.8 %all-gather.3.cloned.1.call-start = ((), (), s32[]{:S(2)}) async-start(), calls=%async_computation.2 | async-start | bytes 1310720 | tf_op jit(solution)/shard_map/all_gather | solution.py:201
  106.7 20.4 %all-to-all-start.1 = ((bf16[8,64,512]{2,1,0:T(8,128)(2,1)}), bf16[8,64,512]{2,1,0:T(8,128)(2,1)S(1)}, u32[]{:S(2)}, u32[]{:S(2)}) async-start(bf16[8,64,512]{2,1,0:T(8,128)(2,1)} %bitcast.12), calls=%async_computation.1 | async-start | bytes 1048576 | tf_op jit(solution)/shard_map/all_to_all | solution.py:213
  127.1 0.8 copy-start.1
Sparse Core Ops, SparseCore 0:
  77.1 25.3 all-gather.4
  104.0 16.6 all-gather.2

commit v3 on v2

--- a/solution.py
+++ b/solution.py
@@ -73,21 +73,25 @@
     experts = half_ref.shape[0] - 1
     capacity = slots // experts
     group_size = experts // GROUPS
-    route = [routes_ref[:, j : j + 1] for j in range(TOPK)]
+    t0 = lax.broadcasted_iota(jnp.int32, (rows, rows), 0)
+    t1 = lax.broadcasted_iota(jnp.int32, (rows, rows), 1)
+
+    def column(row):
+        return jnp.sum(jnp.where(t0 == t1, row.astype(F32), 0.0), axis=-1, keepdims=True)
+
+    route = [column(routes_ref[j : j + 1, :]).astype(jnp.int32) for j in range(TOPK)]
     ids = lax.broadcasted_iota(jnp.int32, (rows, experts), 1)
     hot = [(r == ids).astype(F32) for r in route]
-    t0 = lax.broadcasted_iota(jnp.int32, (rows, rows), 0)
-    t1 = lax.broadcasted_iota(jnp.int32, (rows, rows), 1)
     before = jnp.dot(
         (t1 < t0).astype(BF16), sum(hot).astype(BF16), preferred_element_type=F32
     )
-    group_exp = jnp.exp(gl_ref[...])
-    group_prob = group_exp / jnp.sum(group_exp, axis=-1, keepdims=True)
+    group_exp = [jnp.exp(column(gl_ref[g : g + 1, :])) for g in range(GROUPS)]
+    group_sum = sum(group_exp)
     gids = lax.broadcasted_iota(jnp.int32, (rows, GROUPS), 1)
     member = [
         ((r >= gids * group_size) & (r < (gids + 1) * group_size)).astype(F32) for r in route
     ]
-    choice = [jnp.exp(cl_ref[:, j : j + 1]) for j in range(TOPK)]
+    choice = [jnp.exp(column(cl_ref[j : j + 1, :])) for j in range(TOPK)]
     slot_ids = lax.broadcasted_iota(jnp.int32, (rows, slots), 1)
     place = jnp.zeros((rows, slots), F32)
     weight = jnp.zeros((rows, slots), F32)
@@ -98,7 +102,7 @@
             jnp.sum(member[j] * member[i], axis=-1, keepdims=True) * choice[i]
             for i in range(TOPK)
         )
-        prob = jnp.sum(member[j] * group_prob, axis=-1, keepdims=True)
+        prob = sum(member[j][:, g : g + 1] * group_exp[g] for g in range(GROUPS)) / group_sum
         place = place + mark
         weight = weight + mark * (prob * choice[j] / within)
     high = weight.astype(BF16)
@@ -170,7 +174,7 @@
         in_specs=[SM, VM, VM, VM, VM, VM],
         out_specs=(VM, VM),
         cost_estimate=cost(2 * rows * slots * part, 4000000),
-    )(half, expert_tokens, expert_gain[None, :], routes, group_logits, choice_logits)
+    )(half, expert_tokens, expert_gain[None, :], routes.T, group_logits.T, choice_logits.T)
     arrived = lax.all_to_all(
         outgoing.reshape(experts, capacity, part), "ep", split_axis=0, concat_axis=0, tiled=True
     )
@@ -187,6 +191,7 @@
         out_specs=(VM, VM, VM),
         cost_estimate=cost(3000000000, 4000000),
     )(mixer_query, mixer_forget, mixer_value, forget_floor[None, :])
+    arrived, pay = lax.optimization_barrier((arrived, pay))
     entering = prefix(pay, experts)
     mixed = pl.pallas_call(
         finish_kernel,
@@ -196,9 +201,8 @@
         out_specs=VM,
         cost_estimate=cost(1000000000, 4000000),
     )(entering, intra, qexp, mixer_gate, head_gain[None, :])
-
-    arrived, mixed = lax.optimization_barrier((arrived, mixed))
     mixed_all = lax.all_gather(mixed, "tp", axis=1, tiled=True)
+
     own = arrived.reshape(slots, part)
     other = lax.ppermute(own, "tp", [(i, i ^ 1) for i in range(tp)])
     flat_in = jnp.concatenate(

time: 137 us -> 112 us (0.82)
  starting transfers between devices: 40.1 us -> 26.7 us
  waiting for transfers between devices: 48.7 us -> 42.5 us
  local copies, waits for them, and re-layouts: 6.81 us -> 1.68 us
    all_gather x1, waiting for transfers between devices: 24.7 us -> 0.02 us  [per_device(): hidden_all = lax.all_gather(hidden, 'tp', axis=1, tiled=True)]
    all_to_all x1, waiting for transfers between devices: 0.01 us -> 20.6 us  [per_device(): lax.all_to_all(outgoing.reshape(experts, capacity, part), 'ep', split_axi...]
    ppermute x3, starting transfers between devices: 27.3 us -> 11.6 us  [prefix(): lax.ppermute(span, 'ep', [(i, i + step) for i in range(count - step)])]
    unnamed x9 -> x8, local copies, waits for them, and re-layouts: 5.52 us -> 1.15 us
    all_to_all x1, starting transfers between devices: 5.51 us -> 7.78 us  [per_device(): lax.all_to_all(down.reshape(experts, capacity, -1), 'ep', split_axis=0, c...]
  transfers between devices with their start and end apart: 8 -> 8, of which waited for: 7 -> 7; matrix products, arithmetic and copies ran while one was open for 7% -> 8% of each run, Pallas kernels for 6% -> 7%
where the time goes in v3:
time: 112 us; the launch traced here: 111 us
  waiting for transfers between devices  42.5 us (38%)
  starting transfers between devices  26.7 us (24%)
  between operations  14.2 us (13%)
  Pallas kernels  12.7 us (11%)
  matrix products  11 us (10%)
  other arithmetic  2.37 us (2%)
  local copies, waits for them, and re-layouts  1.68 us (2%)
    all_to_all x1, waiting for transfers between devices, per_device(): lax.all_to_all(outgoing.reshape(experts, capacity, part), 'ep', split_axi...  20.6 us
    ppermute x3, starting transfers between devices, prefix(): lax.ppermute(span, 'ep', [(i, i + step) for i in range(count - step)])  11.6 us
    ppermute x3, waiting for transfers between devices, prefix(): lax.ppermute(span, 'ep', [(i, i + step) for i in range(count - step)])  8.36 us
    all_gather x1, waiting for transfers between devices, per_device(): mixed_all = lax.all_gather(mixed, 'tp', axis=1, tiled=True)  8.01 us
    all_to_all x1, starting transfers between devices, per_device(): lax.all_to_all(down.reshape(experts, capacity, -1), 'ep', split_axis=0, c...  7.78 us
    all_to_all x1, starting transfers between devices, per_device(): lax.all_to_all(outgoing.reshape(experts, capacity, part), 'ep', split_axi...  7.28 us
    pallas_call x1, Pallas kernels, per_device(): pl.pallas_call(local_kernel, name='local_scan', out_shape=(shaped((length...  5.13 us
    dot_general x1, matrix products, per_device(): jnp.dot(hidden_all, w_down[0], preferred_element_type=F32).astype(BF16)  4.26 us
  transfers between devices with their start and end apart: 8, of which 7 were waited for; matrix products, arithmetic and copies ran while one was open for 8% of the time, Pallas kernels for 7%

profile of v3, /device:TPU:0, one launch (start us, length us, event | category | flops | bytes accessed | tf_op | source)
XLA Modules:
  0.0 111.2 jit_solution(13398230420160067331)
XLA Ops:
  7.2 0.5 add.24.half_ref
  7.7 3.1 %dispatch.1 = (bf16[512,1024]{1,0:T(8,128)(2,1)}, bf16[2,128,512]{2,1,0:T(8,128)(2,1)}) custom-call(s32[9]{0:T(128)} %add.24.half_ref, bf16[128,2048]{1,0:T(8,128)(2,1)} %x_ref.1, f32[1,2048]{1,0:T(1,128)} %bitcast.35, s32[2,128]{1,0:T(2,128)} %bitcast.41, f32[4,128]{1,0:T(4,128)} %bitcast.40, f32[2,128]{1,0:T(2,128)} %bitcast.42), custom_call_target="tpu_custom_call" | custom-call | flops 134217728 | bytes 4000000 | tf_op jit(solution)/shard_map/dispatch/pallas_call | solution.py:170
  10.8 7.3 %all-to-all-start = ((bf16[8,64,1024]{2,1,0:T(8,128)(2,1)}), bf16[8,64,1024]{2,1,0:T(8,128)(2,1)S(1)}, u32[]{:S(2)}, u32[]{:S(2)}) async-start(bf16[8,64,1024]{2,1,0:T(8,128)(2,1)} %bitcast.34), calls=%async_computation | async-start | bytes 2097152 | tf_op jit(solution)/shard_map/all_to_all | solution.py:178
  18.2 5.1 %local_scan.1 = (f32[256,512]{1,0:T(8,128)}, bf16[256,512]{1,0:T(8,128)(2,1)}, bf16[4,136,128]{2,1,0:T(8,128)(2,1)}) custom-call(bf16[256,512]{1,0:T(8,128)(2,1)} %q_ref.1, bf16[256,512]{1,0:T(8,128)(2,1)} %f_ref.1, bf16[256,512]{1,0:T(8,128)(2,1)} %v_ref.1, f32[1,512]{1,0:T(1,128)} %bitcast.43), custom_call_target="tpu_custom_call" | custom-call | flops 3000000000 | bytes 4000000 | tf_op jit(solution)/shard_map/local_scan/pallas_call | solution.py:182
  23.3 20.6 %all-to-all-done = bf16[8,64,1024]{2,1,0:T(8,128)(2,1)S(1)} async-done(((bf16[8,64,1024]{2,1,0:T(8,128)(2,1)}), bf16[8,64,1024]{2,1,0:T(8,128)(2,1)S(1)}, u32[]{:S(2)}, u32[]{:S(2)}) %all-to-all-start) | async-done | bytes 1048608 | tf_op jit(solution)/shard_map/all_to_all | solution.py:178
  43.9 2.8 %collective-permute-done.3 = bf16[512,1024]{1,0:T(8,128)(2,1)} collective-permute-done((bf16[512,1024]{1,0:T(8,128)(2,1)S(1)}, bf16[512,1024]{1,0:T(8,128)(2,1)}, u32[]{:S(2)}, u32[]{:S(2)}) %collective-permute-start.3) | collective-permute-done | bytes 1048608 | tf_op jit(solution)/shard_map/ppermute | solution.py:207
  46.7 1.4 %broadcast_select_fusion.1 = (bf16[512,1024]{1,0:T(8,128)(2,1)S(1)}, bf16[512,1024]{1,0:T(8,128)(2,1)S(1)}) fusion(bf16[512,1024]{1,0:T(8,128)(2,1)} %collective-permute-done.3, pred[]{:T(512)S(6)} %eq.6, bf16[8,64,1024]{2,1,0:T(8,128)(2,1)S(1)} %all-to-all-done), kind=kLoop, calls=%fused_computation.11 | loop fusion | flops 1048576 | bytes 4194305 | tf_op jit(solution)/shard_map/jit(_where)/select_n | solution.py:209
  48.1 1.2 %fusion.4 = f32[512,512]{1,0:T(8,128)S(1)} fusion(bf16[1,2048,512]{2,1,0:T(8,128)(2,1)S(1)} %copy-done, bf16[512,1024]{1,0:T(8,128)(2,1)S(1)} %get-tuple-element.17, bf16[512,1024]{1,0:T(8,128)(2,1)S(1)} %get-tuple-element.16), kind=kOutput, calls=%fused_computation.5 | convolution fusion | flops 1077936128 | bytes 5242880 | tf_op jit(solution)/shard_map/dot_general | solution.py:211
  49.6 2.1 %multiply_convert_fusion = bf16[512,512]{1,0:T(8,128)(2,1)} fusion(f32[512,512]{1,0:T(8,128)S(1)} %fusion.4, bf16[1,2048,512]{2,1,0:T(8,128)(2,1)S(1)} %copy-done.3, bf16[512,1024]{1,0:T(8,128)(2,1)S(1)} %get-tuple-element.17, bf16[512,1024]{1,0:T(8,128)(2,1)S(1)} %get-tuple-element.16), kind=kOutput, calls=%fused_computation.9 | convolution fusion | flops 1079508992 | bytes 5767168 | tf_op jit(solution)/shard_map/dot_general | solution.py:212
  51.9 3.3 %collective-permute-start = (bf16[4,136,128]{2,1,0:T(8,128)(2,1)S(1)}, bf16[4,136,128]{2,1,0:T(8,128)(2,1)S(1)}, u32[]{:S(2)}, u32[]{:S(2)}) collective-permute-start(bf16[4,136,128]{2,1,0:T(8,128)(2,1)S(1)} %copy-done.2), channel_id=1, source_target_pairs={{0,4},{4,8},{8,12},{12,16},{16,20},{20,24},{24,28},{1,5},{5,9},{9,... | collective-permute-start | bytes 417800 | tf_op jit(solution)/shard_map/ppermute | solution.py:138
  55.2 3.2 %collective-permute-done = bf16[4,136,128]{2,1,0:T(8,128)(2,1)S(1)} collective-permute-done((bf16[4,136,128]{2,1,0:T(8,128)(2,1)S(1)}, bf16[4,136,128]{2,1,0:T(8,128)(2,1)S(1)}, u32[]{:S(2)}, u32[]{:S(2)}) %collective-permute-start) | collective-permute-done | bytes 139296 | tf_op jit(solution)/shard_map/ppermute | solution.py:138
  58.5 4.1 %collective-permute-start.1 = (bf16[4,136,128]{2,1,0:T(8,128)(2,1)S(1)}, bf16[4,136,128]{2,1,0:T(8,128)(2,1)S(1)}, u32[]{:S(2)}, u32[]{:S(2)}) collective-permute-start(bf16[4,136,128]{2,1,0:T(8,128)(2,1)S(1)} %add_convert_fusion.1), channel_id=1, source_target_pairs={{0,8},{4,12},{8,16},{12,20},{16,24},{20,28},{1,9},{5,13},{9,17},{1... | collective-permute-start | bytes 417800 | tf_op jit(solution)/shard_map/ppermute | solution.py:138
  62.7 2.6 %collective-permute-done.1 = bf16[4,136,128]{2,1,0:T(8,128)(2,1)S(1)} collective-permute-done((bf16[4,136,128]{2,1,0:T(8,128)(2,1)S(1)}, bf16[4,136,128]{2,1,0:T(8,128)(2,1)S(1)}, u32[]{:S(2)}, u32[]{:S(2)}) %collective-permute-start.1) | collective-permute-done | bytes 139296 | tf_op jit(solution)/shard_map/ppermute | solution.py:138
  65.4 4.1 %collective-permute-start.2 = (bf16[4,136,128]{2,1,0:T(8,128)(2,1)S(1)}, bf16[4,136,128]{2,1,0:T(8,128)(2,1)S(1)}, u32[]{:S(2)}, u32[]{:S(2)}) collective-permute-start(bf16[4,136,128]{2,1,0:T(8,128)(2,1)S(1)} %get-tuple-element.18), channel_id=1, source_target_pairs={{0,16},{4,20},{8,24},{12,28},{1,17},{5,21},{9,25},{13,29},{2,18},{... | collective-permute-start | bytes 417800 | tf_op jit(solution)/shard_map/ppermute | solution.py:138
  69.6 2.6 %collective-permute-done.2 = bf16[4,136,128]{2,1,0:T(8,128)(2,1)S(1)} collective-permute-done((bf16[4,136,128]{2,1,0:T(8,128)(2,1)S(1)}, bf16[4,136,128]{2,1,0:T(8,128)(2,1)S(1)}, u32[]{:S(2)}, u32[]{:S(2)}) %collective-permute-start.2) | collective-permute-done | bytes 139296 | tf_op jit(solution)/shard_map/ppermute | solution.py:138
  72.1 0.8 add_convert_fusion.state_ref
  72.9 2.4 %mixer_finish.1 = bf16[256,512]{1,0:T(8,128)(2,1)} custom-call(bf16[4,136,128]{2,1,0:T(8,128)(2,1)} %add_convert_fusion.state_ref, f32[256,512]{1,0:T(8,128)} %get-tuple-element.12.intra_ref, bf16[256,512]{1,0:T(8,128)(2,1)} %get-tuple-element.13.qexp_ref, bf16[256,512]{1,0:T(8,128)(2,1)} %gate_ref.1, f32[1,128]{1,0:T(1,128)} %bitcast.44), custom_call_target="tpu_custom_call" | custom-call | flops 1000000000 | bytes 4000000 | tf_op jit(solution)/shard_map/mixer_finish/pallas_call | solution.py:196
  75.3 4.3 %fusion.6 = bf16[512,512]{1,0:T(8,128)(2,1)} fusion(bf16[512,2048]{1,0:T(8,128)(2,1)} %all-gather.5.cloned.1.call-done, bf16[1,2048,512]{2,1,0:T(8,128)(2,1)} %param.29), kind=kOutput, calls=%fused_computation.7 | convolution fusion | flops 1074003968 | bytes 4718592 | tf_op jit(solution)/shard_map/dot_general | solution.py:216
  79.6 7.8 %all-to-all-start.1 = ((bf16[8,64,512]{2,1,0:T(8,128)(2,1)}), bf16[8,64,512]{2,1,0:T(8,128)(2,1)S(1)}, u32[]{:S(2)}, u32[]{:S(2)}) async-start(bf16[8,64,512]{2,1,0:T(8,128)(2,1)} %bitcast.15), calls=%async_computation.1 | async-start | bytes 1048576 | tf_op jit(solution)/shard_map/all_to_all | solution.py:217
  87.4 8.0 %all-gather.3.cloned.1.call-done = bf16[256,2048]{1,0:T(8,128)(2,1)} async-done(((bf16[256,512]{1,0:T(8,128)(2,1)}), bf16[256,2048]{1,0:T(8,128)(2,1)}) %all-gather.3.cloned.1.call-update) | async-done | bytes 1048592 | tf_op jit(solution)/shard_map/all_gather | solution.py:204
  95.4 3.3 %convolution_convert_fusion = bf16[256,512]{1,0:T(8,128)(2,1)} fusion(bf16[256,2048]{1,0:T(8,128)(2,1)} %all-gather.3.cloned.1.call-done, bf16[2048,512]{1,0:T(8,128)(2,1)} %param.21), kind=kOutput, calls=%fused_computation.8 | convolution fusion | flops 537001984 | bytes 3407872 | tf_op jit(solution)/shard_map/dot_general | solution.py:215
  98.7 2.7 %all-to-all-done.1 = bf16[8,64,512]{2,1,0:T(8,128)(2,1)S(1)} async-done(((bf16[8,64,512]{2,1,0:T(8,128)(2,1)}), bf16[8,64,512]{2,1,0:T(8,128)(2,1)S(1)}, u32[]{:S(2)}, u32[]{:S(2)}) %all-to-all-start.1) | async-done | bytes 524320 | tf_op jit(solution)/shard_map/all_to_all | solution.py:217
  101.4 0.8 copy-done.1
  102.2 2.1 %weigh.1 = bf16[128,512]{1,0:T(8,128)(2,1)} custom-call(bf16[2,128,512]{2,1,0:T(8,128)(2,1)} %get-tuple-element.14.wt_ref, bf16[512,512]{1,0:T(8,128)(2,1)} %bitcast.33), custom_call_target="tpu_custom_call" | custom-call | flops 134217728 | bytes 1000000 | tf_op jit(solution)/shard_map/weigh/pallas_call | solution.py:220
  (20 shorter events, 0.8 us)
Async XLA Ops:
  7.2 40.9 %copy-start = (bf16[1,2048,512]{2,1,0:T(8,128)(2,1)S(1)}, bf16[1,2048,512]{2,1,0:T(8,128)(2,1)}, u32[]{:S(2)}) copy-start(bf16[1,2048,512]{2,1,0:T(8,128)(2,1)} %param.27) | copy-start | bytes 6291460
  10.8 33.0 %all-to-all-start = ((bf16[8,64,1024]{2,1,0:T(8,128)(2,1)}), bf16[8,64,1024]{2,1,0:T(8,128)(2,1)S(1)}, u32[]{:S(2)}, u32[]{:S(2)}) async-start(bf16[8,64,1024]{2,1,0:T(8,128)(2,1)} %bitcast.34), calls=%async_computation | async-start | bytes 2097152 | tf_op jit(solution)/shard_map/all_to_all | solution.py:178
  18.1 57.2 %all-gather.5.cloned.1.call-start = ((), (), s32[]{:S(2)}) async-start(), calls=%async_computation.3 | async-start | bytes 2621440 | tf_op jit(solution)/shard_map/all_gather | solution.py:214
  43.9 2.8 %collective-permute-start.3 = (bf16[512,1024]{1,0:T(8,128)(2,1)S(1)}, bf16[512,1024]{1,0:T(8,128)(2,1)}, u32[]{:S(2)}, u32[]{:S(2)}) collective-permute-start(bf16[512,1024]{1,0:T(8,128)(2,1)S(1)} %bitcast.32), channel_id=1, source_target_pairs={{0,1},{1,0},{2,3},{3,2},{4,5},{5,4},{6,7},{7,6},{8,9},{9,8},{10,11... | collective-permute-start | bytes 3145736 | tf_op jit(solution)/shard_map/ppermute | solution.py:207
  48.1 1.6 %copy-start.3 = (bf16[1,2048,512]{2,1,0:T(8,128)(2,1)S(1)}, bf16[1,2048,512]{2,1,0:T(8,128)(2,1)}, u32[]{:S(2)}) copy-start(bf16[1,2048,512]{2,1,0:T(8,128)(2,1)} %param.28) | copy-start | bytes 6291460
  49.6 2.2 %copy-start.2 = (bf16[4,136,128]{2,1,0:T(8,128)(2,1)S(1)}, bf16[4,136,128]{2,1,0:T(8,128)(2,1)}, u32[]{:S(2)}) copy-start(bf16[4,136,128]{2,1,0:T(8,128)(2,1)} %get-tuple-element.11) | copy-start | bytes 417796
  51.8 43.6 %all-gather.3.cloned.1.call-start = ((), (), s32[]{:S(2)}) async-start(), calls=%async_computation.2 | async-start | bytes 1310720 | tf_op jit(solution)/shard_map/all_gather | solution.py:204
  51.9 6.6 %collective-permute-start = (bf16[4,136,128]{2,1,0:T(8,128)(2,1)S(1)}, bf16[4,136,128]{2,1,0:T(8,128)(2,1)S(1)}, u32[]{:S(2)}, u32[]{:S(2)}) collective-permute-start(bf16[4,136,128]{2,1,0:T(8,128)(2,1)S(1)} %copy-done.2), channel_id=1, source_target_pairs={{0,4},{4,8},{8,12},{12,16},{16,20},{20,24},{24,28},{1,5},{5,9},{9,... | collective-permute-start | bytes 417800 | tf_op jit(solution)/shard_map/ppermute | solution.py:138
  58.5 6.8 %collective-permute-start.1 = (bf16[4,136,128]{2,1,0:T(8,128)(2,1)S(1)}, bf16[4,136,128]{2,1,0:T(8,128)(2,1)S(1)}, u32[]{:S(2)}, u32[]{:S(2)}) collective-permute-start(bf16[4,136,128]{2,1,0:T(8,128)(2,1)S(1)} %add_convert_fusion.1), channel_id=1, source_target_pairs={{0,8},{4,12},{8,16},{12,20},{16,24},{20,28},{1,9},{5,13},{9,17},{1... | collective-permute-start | bytes 417800 | tf_op jit(solution)/shard_map/ppermute | solution.py:138
  65.4 6.7 %collective-permute-start.2 = (bf16[4,136,128]{2,1,0:T(8,128)(2,1)S(1)}, bf16[4,136,128]{2,1,0:T(8,128)(2,1)S(1)}, u32[]{:S(2)}, u32[]{:S(2)}) collective-permute-start(bf16[4,136,128]{2,1,0:T(8,128)(2,1)S(1)} %get-tuple-element.18), channel_id=1, source_target_pairs={{0,16},{4,20},{8,24},{12,28},{1,17},{5,21},{9,25},{13,29},{2,18},{... | collective-permute-start | bytes 417800 | tf_op jit(solution)/shard_map/ppermute | solution.py:138
  79.6 21.8 %all-to-all-start.1 = ((bf16[8,64,512]{2,1,0:T(8,128)(2,1)}), bf16[8,64,512]{2,1,0:T(8,128)(2,1)S(1)}, u32[]{:S(2)}, u32[]{:S(2)}) async-start(bf16[8,64,512]{2,1,0:T(8,128)(2,1)} %bitcast.15), calls=%async_computation.1 | async-start | bytes 1048576 | tf_op jit(solution)/shard_map/all_to_all | solution.py:217
  101.4 0.8 copy-start.1
Sparse Core Ops, SparseCore 0:
  51.9 21.5 all-gather.4
  75.4 19.9 all-gather.2
